TPU v7x, 256 devices: a whole 4x4x8 slice. The times are simulated.
256 devices in a mesh: sp: 64 (over z, x, core), tp: 4 (over y).
Axes of the slice: x: 4, y: 4, z: 8, core: 2. Of those that a mesh axis runs over, the one named last changes fastest.
Arguments:
- layer_input: bfloat16 [8192, 2048], P('sp', 'tp'), may hold values from -6 to 6
- cotangent: bfloat16 [8192, 2048], P('sp', 'tp'), may hold values from -16 to 16
- routes: int32 [8192, 2], P('sp'), may hold values from 0 to 63, all different within a row; in each aligned block of 128 rows (0 to 127, 128 to 255, ...) at most 6 rows name the same one
- route_weight: float32 [8192, 2], P('sp'), may hold values from 0.1 to 0.6
- gate_weight: bfloat16 [64, 2048, 1024], P('sp', None, 'tp'), may hold values from -0.125 to 0.125
- up_weight: bfloat16 [64, 2048, 1024], P('sp', None, 'tp'), may hold values from -0.125 to 0.125
- down_weight: bfloat16 [64, 1024, 2048], P('sp', 'tp'), may hold values from -0.1875 to 0.1875
- heads_value: bfloat16 [8192, 2048], P('sp', 'tp'), may hold values from -6 to 6
- output_gate: bfloat16 [8192, 2048], P('sp', 'tp'), may hold values from -8 to 8
- mixer_saved: bfloat16 [8192, 2048], P('sp', 'tp'), may hold values from -6 to 6
- proj_weight: bfloat16 [2048, 2048], P(None, 'tp'), may hold values from -0.125 to 0.125
- state_write: bfloat16 [8192, 512], P('sp', 'tp'), may hold values from -0.5 to 0.5
- state_read: bfloat16 [8192, 512], P('sp', 'tp'), may hold values from -0.5 to 0.5
- decay_rate: float32 [8192, 32], P('sp', 'tp'), may hold values from 0 to 1.1, as said below
Outputs:
- gate_grad: bfloat16 [64, 2048, 1024], P('sp', None, 'tp')
- up_grad: bfloat16 [64, 2048, 1024], P('sp', None, 'tp')
- down_grad: bfloat16 [64, 1024, 2048], P('sp', 'tp')
- proj_grad: float32 [2048, 2048], P('sp', 'tp')
- value_grad: bfloat16 [8192, 2048], P('sp', 'tp')
- write_gradient: bfloat16 [8192, 512], P('sp', 'tp')
- read_gradient: bfloat16 [8192, 512], P('sp', 'tp')
- outgate_grad: bfloat16 [8192, 2048], P('sp', 'tp')
Inputs may be any that keep to these rules, and one draw needn't show every extreme that they name: `routes`: each row names 2 different experts; within the rows of one aligned block of 128 tokens no expert is named by more than 6 rows, a bound that some block reaches. `decay_rate`: positive log-decays.
All inputs are finite; a program needn't handle non-finite values.
Results may differ from a plain program's by a relative error of at most 0.017.
Values may be sent and summed in bfloat16 or wider, within the bound.
A program may use at most 128 MiB of HBM per device.

v0:
```python
import jax
import jax.numpy as jnp
from jax import lax
from jax.sharding import Mesh
from jax.sharding import PartitionSpec as P

HEAD_DIM = 64
STATE = 128
SP = ("sp_0", "sp_1", "sp_2")


maximal_value = lax.Precision.HIGHEST


def in_blocks(x, dim, count):
    dims = x.shape
    pieces = x.reshape(*dims[:dim], count, dims[dim] // count, *dims[dim + 1 :])
    return jnp.moveaxis(pieces, dim, 0)


def summed_on_arrival(x, axis, dim):
    pieces = in_blocks(x, dim, lax.axis_size(axis))
    arrived = lax.all_to_all(pieces, axis, split_axis=0, concat_axis=0, tiled=True)
    return arrived.astype(jnp.float32).sum(axis=0)


def filled_with(x, identity):
    return jax.tree.map(
        lambda a, e: jnp.broadcast_to(jnp.asarray(e, a.dtype), a.shape), x, identity
    )


def prefix_by_axis(x, axes, combine, identity, reverse):
    before = start = filled_with(x, identity)
    subtotal = x
    for axis in reversed(axes):
        count, index = (lax.axis_size(axis), lax.axis_index(axis))
        pieces = jax.tree.map(
            lambda part, kind: lax.all_gather(part.astype(kind), axis),
            subtotal,
            jax.tree.map(lambda a: jnp.bfloat16 if a.dtype == jnp.float32 else a.dtype, x),
        )
        inside, subtotal = (start, start)
        for k in reversed(range(count)) if reverse else range(count):
            passed = k > index if reverse else k < index
            subtotal = combine(
                subtotal, jax.tree.map(lambda part, own: part[k].astype(own.dtype), pieces, x)
            )
            inside = jax.tree.map(lambda new, old: jnp.where(passed, new, old), subtotal, inside)
        before = combine(inside, before)
    return before


def silu_parts(value):
    sigma = jax.nn.sigmoid(value)
    return (value * sigma, sigma * (1.0 + value * (1.0 - sigma)))


def merge_states(earlier, later):
    fade = jnp.exp(-later[0])[:, :, None, None]
    return (earlier[0] + later[0], fade * earlier[1] + later[1], fade * earlier[2] + later[2])


def on_device(
    layer_input,
    cotangent,
    routes,
    route_weight,
    gate_weight,
    up_weight,
    down_weight,
    heads_value,
    output_gate,
    mixer_saved,
    proj_weight,
    state_write,
    state_read,
    decay_rate,
):
    devices_sp = lax.axis_size(SP)
    local_tokens = layer_input.shape[0]
    top_count = routes.shape[1]
    capacity = max(2, 3 * local_tokens * top_count // (2 * devices_sp))
    flat_routes = routes.reshape(-1)
    onehot = (flat_routes[:, None] == jnp.arange(devices_sp, dtype=jnp.int32)[None, :]).astype(
        jnp.int32
    )
    before = jnp.cumsum(onehot, axis=0, dtype=jnp.int32) - onehot
    ranks = jnp.sum(before * onehot, axis=1, dtype=jnp.int32)
    slots = flat_routes * capacity + ranks
    owners = jnp.arange(flat_routes.shape[0], dtype=jnp.int32) // top_count
    slot_owner = jnp.full((devices_sp * capacity,), local_tokens, jnp.int32).at[slots].set(owners)
    slot_weight = (
        jnp.zeros((devices_sp * capacity,), jnp.float32).at[slots].set(route_weight.reshape(-1))
    )

    def fill_slots(rows):
        padded = jnp.concatenate([rows, jnp.zeros((1, rows.shape[1]), rows.dtype)], axis=0)
        return jnp.take(padded, slot_owner, axis=0)

    part_input = lax.all_to_all(
        fill_slots(layer_input), SP, split_axis=0, concat_axis=0, tiled=True
    )
    part_cotangent = lax.all_to_all(
        (fill_slots(cotangent).astype(jnp.float32) * slot_weight[:, None]).astype(jnp.bfloat16),
        SP,
        split_axis=0,
        concat_axis=0,
        tiled=True,
    )
    expert_input, expert_cotangent = (
        lax.all_gather(part_input, "tp", axis=1, tiled=True),
        lax.all_gather(part_cotangent, "tp", axis=1, tiled=True),
    )
    contract_last = (((1,), (1,)), ((), ()))
    contract_first = (((0,), (0,)), ((), ()))
    gate_local = gate_weight[0]
    up_local = up_weight[0]
    down_local = down_weight[0]
    pre_gate = jnp.dot(expert_input, gate_local, preferred_element_type=jnp.float32)
    pre_up = jnp.dot(expert_input, up_local, preferred_element_type=jnp.float32)
    active, slope = silu_parts(pre_gate)
    hidden = (active * pre_up).astype(jnp.bfloat16)
    hidden_grad = lax.dot_general(
        expert_cotangent, down_local, contract_last, preferred_element_type=jnp.float32
    )
    gate_delta = (hidden_grad * pre_up * slope).astype(jnp.bfloat16)
    up_delta = (hidden_grad * active).astype(jnp.bfloat16)
    down_grad = lax.dot_general(
        hidden, expert_cotangent, contract_first, preferred_element_type=jnp.float32
    ).astype(jnp.bfloat16)[None]
    gate_grad = lax.dot_general(
        expert_input, gate_delta, contract_first, preferred_element_type=jnp.float32
    ).astype(jnp.bfloat16)[None]
    up_grad = lax.dot_general(
        expert_input, up_delta, contract_first, preferred_element_type=jnp.float32
    ).astype(jnp.bfloat16)[None]
    partial_grad = lax.dot_general(
        gate_delta, gate_local, contract_last, preferred_element_type=jnp.float32
    )
    partial_grad = partial_grad + lax.dot_general(
        up_delta, up_local, contract_last, preferred_element_type=jnp.float32
    )
    rounded = lax.optimization_barrier(partial_grad.astype(jnp.bfloat16)).astype(jnp.float32)
    returned = lax.psum_scatter(rounded.astype(jnp.bfloat16), "tp", scatter_dimension=1, tiled=True)
    arrived = lax.all_to_all(returned, SP, split_axis=0, concat_axis=0, tiled=True)
    moe_grad = (
        jnp.take(arrived, slots, axis=0)
        .astype(jnp.float32)
        .reshape(local_tokens, top_count, -1)
        .sum(axis=1)
    )
    layer_grad = (cotangent.astype(jnp.float32) + moe_grad).astype(jnp.bfloat16)
    full_grad = lax.all_gather(layer_grad, "tp", axis=1, tiled=True)
    out_delta = jnp.dot(full_grad, proj_weight, preferred_element_type=jnp.float32).astype(
        jnp.bfloat16
    )
    active_gate, slope_gate = silu_parts(output_gate.astype(jnp.float32))
    saved = mixer_saved.astype(jnp.float32)
    gated = (saved * active_gate).astype(jnp.bfloat16)
    proj_grad = summed_on_arrival(
        lax.dot_general(
            full_grad, gated, contract_first, preferred_element_type=jnp.float32
        ).astype(jnp.bfloat16),
        SP,
        0,
    )
    outgate_grad = (out_delta.astype(jnp.float32) * saved * slope_gate).astype(jnp.bfloat16)
    mixer_delta = out_delta.astype(jnp.float32) * active_gate
    heads_here = decay_rate.shape[1]
    groups_here = state_write.shape[1] // STATE
    repeat = heads_here // groups_here
    value_vectors = heads_value.astype(jnp.float32).reshape(
        local_tokens, groups_here, repeat, HEAD_DIM
    )
    step_deltas = mixer_delta.reshape(local_tokens, groups_here, repeat, HEAD_DIM)
    write_vectors = state_write.astype(jnp.float32).reshape(local_tokens, groups_here, STATE)
    read_vectors = state_read.astype(jnp.float32).reshape(local_tokens, groups_here, STATE)
    cumul = jnp.cumsum(decay_rate, axis=0).reshape(local_tokens, groups_here, repeat)
    total = cumul[-1]
    fades = jnp.stack([jnp.exp(cumul - total), jnp.exp(-cumul)])[..., None]
    value_sides = value_vectors[None] * fades
    delta_sides = step_deltas[None] * fades
    write_states = jnp.einsum(
        "tgn,ktgrp->kgrnp", write_vectors, value_sides, precision=maximal_value
    )
    read_states = jnp.einsum("tgn,ktgrp->kgrnp", read_vectors, delta_sides, precision=maximal_value)
    lower = (total, write_states[0], read_states[0])
    upper = (total, write_states[1], read_states[1])
    empty = (jnp.zeros_like(total), jnp.zeros_like(lower[1]), jnp.zeros_like(lower[2]))
    _, write_low, read_low = prefix_by_axis(lower, SP, merge_states, empty, False)
    _, write_high, read_high = prefix_by_axis(upper, SP, merge_states, empty, True)
    write_pair = jnp.stack([write_high, write_low])
    read_pair = jnp.stack([read_high, read_low])
    cumul_major = cumul.transpose(1, 2, 0)
    mixing_kernel = jnp.exp(-jnp.abs(cumul_major[..., :, None] - cumul_major[..., None, :]))
    common_part = jnp.einsum("tgn,sgn->gts", read_vectors, write_vectors, precision=maximal_value)
    match_scores = jnp.einsum(
        "olmz,ulmz->lmou", step_deltas, value_vectors, precision=maximal_value
    )
    weighted_values = mixing_kernel * match_scores
    value_grad = jnp.einsum(
        "mevw,vmeq->wmeq",
        mixing_kernel * common_part[:, None],
        step_deltas,
        precision=maximal_value,
    )
    value_grad = value_grad + jnp.sum(
        jnp.einsum("tgn,kgrnp->ktgrp", write_vectors, read_pair, precision=maximal_value) * fades,
        axis=0,
    )
    write_gradient = jnp.einsum(
        "eqcm,ceo->meo", weighted_values, read_vectors, precision=maximal_value
    )
    write_gradient = write_gradient + jnp.einsum(
        "kgrnp,ktgrp->tgn", read_pair, value_sides, precision=maximal_value
    )
    read_gradient = jnp.einsum(
        "yvfk,kyb->fyb", weighted_values, write_vectors, precision=maximal_value
    )
    read_gradient = read_gradient + jnp.einsum(
        "kgrnp,ktgrp->tgn", write_pair, delta_sides, precision=maximal_value
    )
    return (
        gate_grad,
        up_grad,
        down_grad,
        proj_grad,
        value_grad.reshape(local_tokens, -1).astype(jnp.bfloat16),
        write_gradient.reshape(local_tokens, -1).astype(jnp.bfloat16),
        read_gradient.reshape(local_tokens, -1).astype(jnp.bfloat16),
        outgate_grad,
    )


def solution(mesh):
    split = Mesh(mesh.devices.reshape(8, 4, 2, mesh.shape["tp"]), ("sp_0", "sp_1", "sp_2", "tp"))
    placed = (
        P(SP, "tp"),
        P(SP, "tp"),
        P(SP, None),
        P(SP, None),
        P(SP, None, "tp"),
        P(SP, None, "tp"),
        P(SP, "tp", None),
        P(SP, "tp"),
        P(SP, "tp"),
        P(SP, "tp"),
        P(None, "tp"),
        P(SP, "tp"),
        P(SP, "tp"),
        P(SP, "tp"),
    )
    return jax.shard_map(
        on_device,
        mesh=split,
        in_specs=placed,
        out_specs=(
            P(SP, None, "tp"),
            P(SP, None, "tp"),
            P(SP, "tp", None),
            P(SP, "tp"),
            P(SP, "tp"),
            P(SP, "tp"),
            P(SP, "tp"),
            P(SP, "tp"),
        ),
        check_vma=False,
    )
```

profile of v0, /device:TPU:24, one launch (start us, length us, event | category | flops | bytes accessed | tf_op | source)
XLA Modules:
  0.0 397.5 jit_solution(12084770395777683503)
XLA Ops:
  15.1 29.4 %all_to_all.41 = bf16[64,6,512]{2,1,0:T(8,128)(2,1)S(1)} all-to-all(bf16[64,6,512]{2,1,0:T(8,128)(2,1)S(1)} %all_to_all.27), channel_id=1, replica_groups=mesh['sp_0'=8,'sp_1'=4,'sp_2'=2,'tp'=4] {'sp_0','sp_1','sp_2'}, dimensions={0} | all-to-all | bytes 786432 | tf_op jit(solution)/shard_map/all_to_all | solution.py:101
  49.5 23.2 %all_to_all.42 = bf16[64,6,512]{2,1,0:T(8,128)(2,1)S(1)} all-to-all(bf16[64,6,512]{2,1,0:T(8,128)(2,1)S(1)} %all_to_all.30), channel_id=1, replica_groups=mesh['sp_0'=8,'sp_1'=4,'sp_2'=2,'tp'=4] {'sp_0','sp_1','sp_2'}, dimensions={0} | all-to-all | bytes 786432 | tf_op jit(solution)/shard_map/all_to_all | solution.py:104
  73.7 3.2 fusion.19
  78.2 23.2 %all-gather.11.cloned.1.call-done = bf16[384,2048]{1,0:T(8,128)(2,1)} async-done(((bf16[384,512]{1,0:T(8,128)(2,1)}), bf16[384,2048]{1,0:T(8,128)(2,1)}) %all-gather.11.cloned.1.call-update) | async-done | bytes 1572880 | tf_op jit(solution)/shard_map/all_gather | solution.py:113
  110.5 9.6 %all_gather.84 = bf16[4,1,8]{2,1,0:T(2,128)(2,1)S(1)} all-gather(bf16[1,1,8]{2,1,0:T(2,128)(2,1)S(1)} %get-tuple-element.89), channel_id=1, replica_groups=mesh['sp_0'=8,'sp_1'=4,'sp_2'=2,'tp'=4] {'sp_1'}, dimensions={0}, use_global_device_ids=true | all-gather | bytes 80 | tf_op jit(solution)/shard_map/all_gather | solution.py:39
  122.5 12.9 %reduce-scatter.2.cloned.1.call-done = bf16[384,512]{1,0:T(8,128)(2,1)} async-done(((bf16[384,2048]{1,0:T(8,128)(2,1)}), bf16[384,512]{1,0:T(8,128)(2,1)}) %reduce-scatter.2.cloned.1.call-update) | async-done | bytes 393232 | tf_op jit(solution)/shard_map/reduce_scatter | solution.py:145
  137.3 10.4 %all-to-all-start.2 = ((bf16[64,6,512]{2,1,0:T(8,128)(2,1)}), bf16[64,6,512]{2,1,0:T(8,128)(2,1)S(1)}, u32[]{:S(2)}, u32[]{:S(2)}) async-start(bf16[64,6,512]{2,1,0:T(8,128)(2,1)} %all_to_all.33), calls=%async_computation.3 | async-start | bytes 1048576 | tf_op jit(solution)/shard_map/all_to_all | solution.py:146
  151.7 13.6 %all-to-all-done.2 = bf16[64,6,512]{2,1,0:T(8,128)(2,1)S(1)} async-done(((bf16[64,6,512]{2,1,0:T(8,128)(2,1)}), bf16[64,6,512]{2,1,0:T(8,128)(2,1)S(1)}, u32[]{:S(2)}, u32[]{:S(2)}) %all-to-all-start.2) | async-done | bytes 393248 | tf_op jit(solution)/shard_map/all_to_all | solution.py:146
  167.6 12.8 %all_gather.81 = bf16[128,2048]{1,0:T(8,128)(2,1)S(1)} all-gather(bf16[128,512]{1,0:T(8,128)(2,1)S(1)} %add_convert_fusion.1), channel_id=1, replica_groups=mesh['sp_0'=8,'sp_1'=4,'sp_2'=2,'tp'=4] {'tp'}, dimensions={1}, use_global_device_ids=true | all-gather | bytes 655360 | tf_op jit(solution)/shard_map/all_gather | solution.py:154
  184.4 13.9 %all_gather.97 = bf16[4,1,8,128,64]{3,4,2,1,0:T(8,128)(2,1)S(1)} all-gather(bf16[1,1,8,128,64]{3,4,2,1,0:T(8,128)(2,1)S(1)} %get-tuple-element.85), channel_id=1, replica_groups=mesh['sp_0'=8,'sp_1'=4,'sp_2'=2,'tp'=4] {'sp_1'}, dimensions={0}, use_global_device_ids=true | all-gather | bytes 655360 | tf_op jit(solution)/shard_map/all_gather | solution.py:39
  198.3 13.1 %all_gather.91 = bf16[4,1,8,128,64]{3,4,2,1,0:T(8,128)(2,1)S(1)} all-gather(bf16[1,1,8,128,64]{3,4,2,1,0:T(8,128)(2,1)S(1)} %get-tuple-element.86), channel_id=1, replica_groups=mesh['sp_0'=8,'sp_1'=4,'sp_2'=2,'tp'=4] {'sp_1'}, dimensions={0}, use_global_device_ids=true | all-gather | bytes 655360 | tf_op jit(solution)/shard_map/all_gather | solution.py:39
  217.6 12.9 %all_gather.94 = bf16[4,1,8,128,64]{3,4,2,1,0:T(8,128)(2,1)S(1)} all-gather(bf16[1,1,8,128,64]{3,4,2,1,0:T(8,128)(2,1)S(1)} %get-tuple-element.83), channel_id=1, replica_groups=mesh['sp_0'=8,'sp_1'=4,'sp_2'=2,'tp'=4] {'sp_1'}, dimensions={0}, use_global_device_ids=true | all-gather | bytes 655360 | tf_op jit(solution)/shard_map/all_gather | solution.py:39
  230.5 13.6 %all_gather.87 = bf16[4,1,8,128,64]{3,4,2,1,0:T(8,128)(2,1)S(1)} all-gather(bf16[1,1,8,128,64]{3,4,2,1,0:T(8,128)(2,1)S(1)} %get-tuple-element.84), channel_id=1, replica_groups=mesh['sp_0'=8,'sp_1'=4,'sp_2'=2,'tp'=4] {'sp_1'}, dimensions={0}, use_global_device_ids=true | all-gather | bytes 655360 | tf_op jit(solution)/shard_map/all_gather | solution.py:39
  247.4 3.3 convolution_convert_fusion
  250.6 6.1 %all-to-all-start.3 = ((bf16[64,32,512]{2,1,0:T(8,128)(2,1)}), bf16[64,32,512]{2,1,0:T(8,128)(2,1)}, u32[]{:S(2)}, u32[]{:S(2)}) async-start(bf16[64,32,512]{2,1,0:T(8,128)(2,1)} %bitcast.353), calls=%async_computation.4 | async-start | bytes 4194304 | tf_op jit(solution)/shard_map/all_to_all | solution.py:23
  257.5 66.5 %all_gather.89 = bf16[8,1,8]{2,1,0:T(2,128)(2,1)S(1)} all-gather(bf16[1,1,8]{2,1,0:T(2,128)(2,1)S(1)} %get-tuple-element.76), channel_id=1, replica_groups=mesh['sp_0'=8,'sp_1'=4,'sp_2'=2,'tp'=4] {'sp_0'}, dimensions={0}, use_global_device_ids=true | all-gather | bytes 144 | tf_op jit(solution)/shard_map/all_gather | solution.py:39
  324.0 14.1 %all_gather.85 = bf16[8,1,8]{2,1,0:T(2,128)(2,1)S(1)} all-gather(bf16[1,1,8]{2,1,0:T(2,128)(2,1)S(1)} %get-tuple-element.75), channel_id=1, replica_groups=mesh['sp_0'=8,'sp_1'=4,'sp_2'=2,'tp'=4] {'sp_0'}, dimensions={0}, use_global_device_ids=true | all-gather | bytes 144 | tf_op jit(solution)/shard_map/all_gather | solution.py:39
  342.6 3.1 fusion
  345.8 3.3 fusion.1
  351.6 2.6 add_add_fusion.2
  354.2 2.5 add_add_fusion.3
  363.8 3.1 add_add_fusion
  366.9 17.1 %all-gather.17.cloned.1.call-done = bf16[8,1,8,128,64]{3,4,2,1,0:T(8,128)(2,1)} async-done(((bf16[1,1,8,128,64]{3,4,2,1,0:T(8,128)(2,1)}), bf16[8,1,8,128,64]{3,4,2,1,0:T(8,128)(2,1)}) %all-gather.17.cloned.1.call-update) | async-done | bytes 1048592 | tf_op jit(solution)/shard_map/all_gather | solution.py:39
  388.1 2.5 convert_reduce_fusion
  (203 shorter events, 66.5 us)
Async XLA Ops:
  7.2 173.2 %copy-start = (bf16[2048,512]{1,0:T(8,128)(2,1)S(1)}, bf16[2048,512]{1,0:T(8,128)(2,1)}, u32[]{:S(2)}) copy-start(bf16[2048,512]{1,0:T(8,128)(2,1)} %param.26) | copy-start | bytes 6291460
  7.2 66.5 %all-gather.9.cloned.1.call-start = ((), (), s32[]{:S(2)}) async-start(), calls=%async_computation.5 | async-start | bytes 1966080 | tf_op jit(solution)/shard_map/all_gather | solution.py:112
  14.9 30.5 %copy-start.23 = (bf16[128,512]{1,0:T(8,128)(2,1)S(1)}, bf16[128,512]{1,0:T(8,128)(2,1)}, u32[]{:S(2)}) copy-start(bf16[128,512]{1,0:T(8,128)(2,1)} %param.17) | copy-start | bytes 393220
  45.3 56.1 %all-gather.11.cloned.1.call-start = ((), (), s32[]{:S(2)}) async-start(), calls=%async_computation.6 | async-start | bytes 1966080 | tf_op jit(solution)/shard_map/all_gather | solution.py:113
  73.6 61.8 %reduce-scatter.2.cloned.1.call-start = ((), (), s32[]{:S(2)}) async-start(), calls=%async_computation.7 | async-start | bytes 1966080 | tf_op jit(solution)/shard_map/reduce_scatter | solution.py:145
  78.2 25.8 %copy-start.16 = (bf16[1,2048,256]{2,1,0:T(8,128)(2,1)S(1)}, bf16[1,2048,256]{2,1,0:T(8,128)(2,1)}, u32[]{:S(2)}) copy-start(bf16[1,2048,256]{2,1,0:T(8,128)(2,1)} %param.20) | copy-start | bytes 3145732
  137.3 28.1 %all-to-all-start.2 = ((bf16[64,6,512]{2,1,0:T(8,128)(2,1)}), bf16[64,6,512]{2,1,0:T(8,128)(2,1)S(1)}, u32[]{:S(2)}, u32[]{:S(2)}) async-start(bf16[64,6,512]{2,1,0:T(8,128)(2,1)} %all_to_all.33), calls=%async_computation.3 | async-start | bytes 1048576 | tf_op jit(solution)/shard_map/all_to_all | solution.py:146
  147.7 203.8 %all-gather.15.cloned.1.call-start = ((), (), s32[]{:S(2)}) async-start(), calls=%async_computation.9 | async-start | bytes 1179648 | tf_op jit(solution)/shard_map/all_gather | solution.py:39
  150.4 33.7 %copy-start.4 = (bf16[2,1,8,128,64]{3,4,2,1,0:T(8,128)(2,1)}, bf16[2,1,8,128,64]{3,4,2,1,0:T(8,128)(2,1)S(1)}, u32[]{:S(2)}) copy-start(bf16[2,1,8,128,64]{3,4,2,1,0:T(8,128)(2,1)S(1)} %all_gather.96) | copy-start | bytes 786436
  181.7 169.2 %copy-start.9 = (f32[128,512]{0,1:T(8,128)}, f32[128,512]{0,1:T(8,128)S(1)}, u32[]{:S(2)}) copy-start(f32[128,512]{0,1:T(8,128)S(1)} %copy.135) | copy-start | bytes 786436
  182.1 30.1 %copy-start.33 = (f32[8]{0:T(128)S(1)}, f32[8]{0:T(128)}, u32[]{:S(2)}) copy-start(f32[8]{0:T(128)} %get-tuple-element.82) | copy-start | bytes 100
  182.1 30.1 %copy-start.36 = (f32[8]{0:T(128)S(1)}, f32[8]{0:T(128)}, u32[]{:S(2)}) copy-start(f32[8]{0:T(128)} %get-tuple-element.77) | copy-start | bytes 100
  182.1 30.1 %copy-start.37 = (f32[8]{0:T(128)S(1)}, f32[8]{0:T(128)}, u32[]{:S(2)}) copy-start(f32[8]{0:T(128)} %get-tuple-element.79) | copy-start | bytes 100
  184.3 29.1 %copy-start.21 = (bf16[1,1,8,128,64]{3,4,2,1,0:T(8,128)(2,1)S(1)}, bf16[1,1,8,128,64]{3,4,2,1,0:T(8,128)(2,1)}, u32[]{:S(2)}) copy-start(bf16[1,1,8,128,64]{3,4,2,1,0:T(8,128)(2,1)} %get-tuple-element.49) | copy-start | bytes 393220
  198.3 19.2 %copy-start.38 = (f32[8]{0:T(128)S(1)}, f32[8]{0:T(128)}, u32[]{:S(2)}) copy-start(f32[8]{0:T(128)} %get-tuple-element.88) | copy-start | bytes 100
  198.3 19.2 %copy-start.40 = (f32[8]{0:T(128)S(1)}, f32[8]{0:T(128)}, u32[]{:S(2)}) copy-start(f32[8]{0:T(128)} %get-tuple-element.87) | copy-start | bytes 100
  213.4 140.8 %all-gather.13.cloned.1.call-start = ((), (), s32[]{:S(2)}) async-start(), calls=%async_computation.8 | async-start | bytes 1179648 | tf_op jit(solution)/shard_map/all_gather | solution.py:39
  215.4 15.1 %copy-start.5 = (bf16[2,1,8,128,64]{3,4,2,1,0:T(8,128)(2,1)}, bf16[2,1,8,128,64]{3,4,2,1,0:T(8,128)(2,1)S(1)}, u32[]{:S(2)}) copy-start(bf16[2,1,8,128,64]{3,4,2,1,0:T(8,128)(2,1)S(1)} %all_gather.93) | copy-start | bytes 786436
  246.8 117.1 %all-gather.19.cloned.1.call-start = ((), (), s32[]{:S(2)}) async-start(), calls=%async_computation.11 | async-start | bytes 1179648 | tf_op jit(solution)/shard_map/all_gather | solution.py:39
  250.6 137.5 %all-to-all-start.3 = ((bf16[64,32,512]{2,1,0:T(8,128)(2,1)}), bf16[64,32,512]{2,1,0:T(8,128)(2,1)}, u32[]{:S(2)}, u32[]{:S(2)}) async-start(bf16[64,32,512]{2,1,0:T(8,128)(2,1)} %bitcast.353), calls=%async_computation.4 | async-start | bytes 4194304 | tf_op jit(solution)/shard_map/all_to_all | solution.py:23
  256.8 127.2 %all-gather.17.cloned.1.call-start = ((), (), s32[]{:S(2)}) async-start(), calls=%async_computation.10 | async-start | bytes 1179648 | tf_op jit(solution)/shard_map/all_gather | solution.py:39
  363.0 21.0 %copy-start.6 = (bf16[2,1,8,128,64]{3,4,2,1,0:T(8,128)(2,1)S(1)}, bf16[2,1,8,128,64]{3,4,2,1,0:T(8,128)(2,1)}, u32[]{:S(2)}) copy-start(bf16[2,1,8,128,64]{3,4,2,1,0:T(8,128)(2,1)} %copy-done.5) | copy-start | bytes 786436
  366.9 19.4 %copy-start.11 = (f32[128,512]{0,1:T(8,128)S(1)}, f32[128,512]{0,1:T(8,128)}, u32[]{:S(2)}) copy-start(f32[128,512]{0,1:T(8,128)} %copy-done.9) | copy-start | bytes 786436
  366.9 19.4 %copy-start.15 = (f32[1,1,8,128,64]{3,4,2,0,1:T(8,128)S(1)}, f32[1,1,8,128,64]{3,4,2,0,1:T(8,128)}, u32[]{:S(2)}) copy-start(f32[1,1,8,128,64]{3,4,2,0,1:T(8,128)} %add_add_fusion) | copy-start | bytes 786436
  (32 other events, 146.8 us)
Sparse Core Ops, SparseCore 0:
  45.5 24.5 all-gather.8
  73.7 27.6 all-gather.10
  107.3 28.0 reduce-scatter.1
  213.5 35.1 all-gather.14
  250.9 51.0 all-gather.12
  303.7 38.8 all-gather.18
  345.9 38.0 all-gather.16
where the time goes:
time: 399 us; the launch traced here: 397 us
  blocking collectives  219 us (55%)
  waiting for transfers between devices  67.5 us (17%)
  matrix products  30.6 us (8%)
  other arithmetic  24.9 us (6%)
  local copies, waits for them, and re-layouts  23.9 us (6%)
  starting transfers between devices  16.9 us (4%)
  between operations  14.9 us (4%)
    all_gather x12, blocking collectives, prefix_by_axis(): lax.all_gather(part.astype(kind), axis)  154 us
    all_to_all x1, blocking collectives, on_device(): lax.all_to_all(fill_slots(layer_input), SP, split_axis=0, concat_axis=0,...  29.4 us
    all_gather x1, waiting for transfers between devices, on_device(): lax.all_gather(part_cotangent, 'tp', axis=1, tiled=True)  23.2 us
    all_to_all x1, blocking collectives, on_device(): lax.all_to_all((fill_slots(cotangent).astype(jnp.float32) * slot_weight[:...  23.2 us
    all_gather x4, waiting for transfers between devices, prefix_by_axis(): lax.all_gather(part.astype(kind), axis)  17.1 us
    all_to_all x1, waiting for transfers between devices, on_device(): lax.all_to_all(returned, SP, split_axis=0, concat_axis=0, tiled=True)  13.6 us
    reduce_scatter x1, waiting for transfers between devices, on_device(): lax.psum_scatter(rounded.astype(jnp.bfloat16), 'tp', scatter_dimension=1,...  12.9 us
    all_gather x1, blocking collectives, on_device(): full_grad = lax.all_gather(layer_grad, 'tp', axis=1, tiled=True)  12.8 us
  transfers between devices with their start and end apart: 9, of which 4 were waited for; matrix products, arithmetic and copies ran while one was open for 13% of the time, Pallas kernels for 0%

commit v1 on v0

v1 whole, which is shorter than its diff:
```python
import jax
import jax.numpy as jnp
from jax import lax
from jax.experimental import pallas as pl
from jax.experimental.pallas import tpu as pltpu
from jax.sharding import Mesh
from jax.sharding import PartitionSpec as P

SP = ("sp_0", "sp_1", "sp_2")
NZ, NX, NC, NY = 8, 4, 2, 4
NSP = NZ * NX * NC
PLANE = NX * NC
T = 128
W = 512
HEADS = 8
CAP = 6
BF = jnp.bfloat16
F32 = jnp.float32
ORDER = (0, 1, 7, 2, 6, 3, 5, 4)
MESH_ID = pl.DeviceIdType.MESH
HIGH = lax.Precision.HIGHEST


def dot(a, b, ca=1, cb=0, precision=None):
    return lax.dot_general(
        a, b, (((ca,), (cb,)), ((), ())), preferred_element_type=F32, precision=precision
    )


def iota(shape, dim):
    return lax.broadcasted_iota(jnp.int32, shape, dim)


def body(
    li_h, cot_h, rt_v, rw_v, gw_h, uw_h, dw_h, hv_h, og_h, ms_h, pw_h, sw_h, sr_h, dr_v,
    gg_o, ug_o, dg_o, pg_o, vg_o, wg_o, rg_o, og_o,
    *scratch,
):
    (
        li, cot, gu, dw, hv, og, ms, pw, sw, sr, sx, gy, xm, cm, acc_gu, acc_h, gud, hid, ps,
        own, hl, hr, mrg, nl, nr, ret, rr, comb, lg, od, dl, sstw, sstr, stw, strd, low, high,
        outw, outr, wsw, wsr, fsend, frecv, vfs, vfi, dfs, dfi, fts, lst, lker, vint, lt, rtm,
        ga, pgs, zr, pgown, ow_gu, ow_d, ow_p, ow_v, ow_w, ow_r, ow_o, ld_sem, o_sem, self_sem,
        d_send, d_recv, y_send, yl_recv, yr_recv, yo_recv, rs_send, rs_recv, ret_send, ret_recv,
        lg_send, lg_recv, st_send, st_recv, ga_send, ga_recv, rt_send, rt_recv, z_send, z_recv,

    ) = scratch
    z = lax.axis_index("sp_0")
    x = lax.axis_index("sp_1")
    c = lax.axis_index("sp_2")
    y = lax.axis_index("tp")
    plane = x * NC + c
    me = z * PLANE + plane

    def ahead(dz, p):
        return (
            lax.rem(z + dz, NZ),
            lax.rem(x + p // NC, NX),
            lax.rem(c + p % NC, NC),
        )

    def behind(dz, p):
        return (
            lax.rem(z + NZ - dz, NZ),
            lax.rem(x + NX - p // NC, NX),
            lax.rem(c + p % NC, NC),
        )

    right = (z, x, c, lax.rem(y + 1, NY))
    left = (z, x, c, lax.rem(y + NY - 1, NY))
    opposite = (z, x, c, lax.rem(y + 2, NY))

    def remote(src, dst, ss, rs, dev):
        pltpu.make_async_remote_copy(
            src_ref=src, dst_ref=dst, send_sem=ss, recv_sem=rs, device_id=dev,
            device_id_type=MESH_ID,
        ).start()

    def local(src, dst, sem):
        pltpu.make_async_copy(src, dst, sem).start()

    def wait(ref, sem):
        pltpu.make_async_copy(ref, ref, sem).wait()

    def to_all(send):
        for p in range(1, PLANE):
            send(0, p)

        def step(n, _):
            odd = lax.rem(n, 2)
            dz = odd * ((n + 1) // 2) + (1 - odd) * (NZ - n // 2)
            for p in range(PLANE):
                send(dz, p)
            return 0

        lax.fori_loop(1, NZ, step, 0)

    loads = (
        (li_h, li), (cot_h, cot), (hv_h, hv), (sw_h, sw), (sr_h, sr), (og_h, og), (ms_h, ms),
        (gw_h.at[0], gu.at[:, pl.ds(0, 256)]), (uw_h.at[0], gu.at[:, pl.ds(256, 256)]),
        (dw_h.at[0], dw), (pw_h, pw),
    )
    for n, (a, b) in enumerate(loads):
        local(a, b, ld_sem.at[n])

    def loaded(n):
        wait(loads[n][1], ld_sem.at[n])

    bar = pltpu.get_barrier_semaphore()

    def greet(dev):
        pl.semaphore_signal(bar, inc=1, device_id=dev, device_id_type=MESH_ID)

    to_all(lambda dz, p: greet(ahead(dz, p) + (y,)))
    greet(right)
    greet(left)
    greet(opposite)

    ci = iota((512, T), 0)
    r8 = lax.rem(ci, 8)
    blk = ci // 8
    e = (
        lax.rem(z + blk // PLANE, NZ) * PLANE
        + lax.rem(x + lax.rem(blk // NC, NX), NX) * NC
        + lax.rem(c + lax.rem(blk, NC), NC)
    )
    r0 = jnp.broadcast_to(rt_v[0:1, :], (512, T))
    r1 = jnp.broadcast_to(rt_v[1:2, :], (512, T))
    hit = (r0 == e) | (r1 == e)
    upper = (iota((T, T), 0) < iota((T, T), 1)).astype(F32).astype(BF)
    hitf = jnp.where(hit, 1.0, 0.0)
    rank = dot(hitf.astype(BF), upper).astype(jnp.int32)
    wsel = jnp.where(
        r0 == e, jnp.broadcast_to(rw_v[0:1, :], (512, T)), jnp.broadcast_to(rw_v[1:2, :], (512, T))
    )
    base = hit & (rank == r8) & (r8 < CAP)
    basef = jnp.where(base, 1.0, 0.0)
    extra = [
        jnp.where(hit & (rank == 2 * k + r8 - CAP) & (r8 >= CAP), 1.0, 0.0) for k in range(3)
    ]
    loaded(0)
    loaded(1)
    for k in range(3):
        pick = jnp.concatenate([basef.astype(BF), extra[k].astype(BF)], axis=1)
        rows = jnp.concatenate(
            [
                jnp.concatenate([li[:, 128 * k : 128 * k + 128], cot[:, 128 * k : 128 * k + 128]], axis=1),
                jnp.concatenate([li[:, 384:512], cot[:, 384:512]], axis=1),
            ],
            axis=0,
        )
        got = dot(pick, rows)
        weight = jnp.sum((basef + extra[k]) * wsel, axis=1, keepdims=True)
        sx.at[k].reshape(512, T)[...] = got[:, :128].astype(BF)
        sx.at[3 + k].reshape(512, T)[...] = (got[:, 128:] * weight).astype(BF)

    comb[0] = basef.T.astype(BF)
    for k in range(3):
        comb[1 + k] = extra[k].T.astype(BF)

    pl.semaphore_wait(bar, NSP - 1 + 3)

    def send_x(dz, p):
        j = dz * PLANE + p
        remote(sx.at[:, j], gy.at[0, :, j], d_send, d_recv.at[dz], ahead(dz, p) + (y,))

    local(sx.at[:, 0], gy.at[0, :, 0], self_sem.at[0])
    to_all(send_x)

    loaded(2)
    loaded(3)
    loaded(4)
    upto = (iota((T, T), 0) <= iota((T, T), 1)).astype(F32)
    cum = dot(dr_v[...], upto, precision=HIGH)
    tot = cum[:, 127:128]
    te = jnp.exp(cum - tot)
    ts = jnp.exp(-cum)
    stacked = jnp.concatenate([te, ts, cum, jnp.zeros((T - 24, T), F32)], axis=0)
    tr = stacked.T
    half = iota((T, T), 1) < 64
    for h in range(HEADS):
        fsend[h] = jnp.broadcast_to(jnp.exp(-tot[h : h + 1, :]), (1, T))
        te_c = jnp.broadcast_to(tr[:, h : h + 1], (T, T))
        ts_c = jnp.broadcast_to(tr[:, 8 + h : 9 + h], (T, T))
        fts[h] = jnp.where(half, ts_c, te_c)
        cc = jnp.broadcast_to(tr[:, 16 + h : 17 + h], (T, T))
        cr = jnp.broadcast_to(cum[h : h + 1, :], (T, T))
        lker[h] = jnp.exp(-jnp.abs(cc - cr))

    def doubled(v, h):
        other = pltpu.roll(v, 64, 1)
        return jnp.where(half, v, other) if h % 2 == 0 else jnp.where(half, other, v)

    def sides(chunk_of, first, second):
        for h in range(HEADS):
            v = doubled(chunk_of(h // 2), h)
            f = fts[h]
            second[h] = (v * f).astype(BF)
            first[h] = (v * pltpu.roll(f, 64, 1)).astype(BF)

    sides(lambda k: hv[:, 128 * k : 128 * k + 128].astype(F32), vfs, vfi)

    def states(vectors_t, first, dst):
        for h in range(0, HEADS, 2):
            s = dot(vectors_t, jnp.concatenate([first[h], first[h + 1]], axis=1))
            dst[pl.ds(8 * h, 8)] = s[:, :T].astype(BF).reshape(8, 16, T)
            dst[pl.ds(8 * h + 8, 8)] = s[:, T:].astype(BF).reshape(8, 16, T)

    swt = sw[...].astype(F32).T.astype(BF)
    states(swt, vfs, sstw)

    def send_state(src, dst, n):
        def go(dz, p):
            zz, xx, cc = ahead(dz, p)
            j = dz * PLANE + p
            remote(src.at[zz * PLANE + xx * NC + cc], dst.at[j], st_send.at[n], st_recv.at[n], (zz, xx, cc, y))

        local(src.at[me], dst.at[0], self_sem.at[1 + n])
        to_all(go)

    def send_fade(dz, p):
        zz, xx, cc = ahead(dz, p)
        j = dz * PLANE + p
        remote(fsend.at[zz], frecv.at[j], st_send.at[4], st_recv.at[4], (zz, xx, cc, y))

    local(fsend.at[z], frecv.at[0], self_sem.at[5])
    to_all(send_fade)
    send_state(sstw, stw, 0)

    loaded(5)
    loaded(6)
    ogf = og[...].astype(F32)
    sig = jax.nn.sigmoid(ogf)
    ga[0] = (ms[...].astype(F32) * (ogf * sig)).astype(BF)
    for p in range(1, PLANE):
        remote(ga.at[0], ga.at[p], ga_send, ga_recv, ahead(0, p) + (y,))

    def chunk(d, dz):
        return gy.at[d, :, pl.ds(PLANE * dz, PLANE)]

    def forward(n):
        dz = ORDER[n]
        if n % 2 == 0:
            wait(chunk(1, dz), yl_recv.at[n])
            remote(chunk(1, dz), chunk(2, dz), y_send, yo_recv.at[n], right)
        else:
            wait(chunk(3, dz), yr_recv.at[n])
            remote(chunk(3, dz), chunk(2, dz), y_send, yo_recv.at[n], left)

    for n, dz in enumerate(ORDER):
        if dz == 0:
            wait(gy.at[0, :, pl.ds(1, PLANE - 1)], d_recv.at[0])
            wait(gy.at[0, :, 0], self_sem.at[0])
        else:
            wait(chunk(0, dz), d_recv.at[dz])
        remote(chunk(0, dz), chunk(1, dz), y_send, yl_recv.at[n], right)
        remote(chunk(0, dz), chunk(3, dz), y_send, yr_recv.at[n], left)
        if n >= 1:
            forward(n - 1)

    r3 = iota((64, 8, T), 1)

    def assemble(d, first, dst):
        last = None
        for k in range(3):
            dst[:, pl.ds(512 * d + 128 * k, 128)] = gy.at[d, first + k].reshape(512, T)[...]
            moved = pltpu.roll(gy[d, first + k].astype(F32), 2 * k + 2, 1)
            last = moved if k == 0 else jnp.where(r3 // 2 == k, moved, last)
        dst[:, pl.ds(512 * d + 384, 128)] = last.reshape(512, T).astype(BF)

    def rows_of(d):
        return pl.multiple_of(lax.rem(y + NY - d, NY) * 512, 512)

    def expert_in(d, start):
        assemble(d, 0, xm)
        assemble(d, 3, cm)
        off = rows_of(d)

        def step(m, _):
            rows = pl.ds(pl.multiple_of(m * 256, 256), 256)
            a = dot(xm[rows, pl.ds(512 * d, 512)], gu[pl.ds(off, 512), :])
            b = dot(cm[rows, pl.ds(512 * d, 512)], dw[:, pl.ds(off, 512)], 1, 1)
            if start:
                acc_gu[rows, :] = a
                acc_h[rows, :] = b
            else:
                acc_gu[rows, :] += a
                acc_h[rows, :] += b
            return 0

        lax.fori_loop(0, 2, step, 0)

    loaded(7)
    loaded(8)
    loaded(9)
    forward(7)
    expert_in(0, True)
    for n in range(8):
        if n % 2 == 1:
            wait(chunk(1, ORDER[n]), yl_recv.at[n])
    expert_in(1, False)
    for n in range(8):
        if n % 2 == 0:
            wait(chunk(3, ORDER[n]), yr_recv.at[n])
    expert_in(3, False)
    for n in range(8):
        wait(chunk(2, ORDER[n]), yo_recv.at[n])
    expert_in(2, False)

    def middle(m, _):
        rows = pl.ds(pl.multiple_of(m * 64, 64), 64)
        keep = lax.rem(iota((64, 256), 0), 8) < CAP
        g = acc_gu[rows, pl.ds(0, 256)]
        u = acc_gu[rows, pl.ds(256, 256)]
        hg = acc_h[rows, :]
        s = jax.nn.sigmoid(g)
        act = g * s
        slope = s * (1.0 + g * (1.0 - s))
        hid[rows, :] = jnp.where(keep, act * u, 0.0).astype(BF)
        gud[rows, pl.ds(0, 256)] = jnp.where(keep, hg * u * slope, 0.0).astype(BF)
        gud[rows, pl.ds(256, 256)] = jnp.where(keep, hg * act, 0.0).astype(BF)
        return 0

    lax.fori_loop(0, 8, middle, 0)

    def packed(d, put):
        off = rows_of(d)

        def step(m, _):
            rows = pl.ds(pl.multiple_of(m * 128, 128), 128)
            a = dot(gud[rows, :], gu[pl.ds(off, 512), :], 1, 1)
            tail = a[:, 384:512].reshape(16, 8, T)
            rr3 = iota((16, 8, T), 1)
            for k in range(3):
                main = a[:, 128 * k : 128 * k + 128].reshape(16, 8, T)
                put(k, m, jnp.where(rr3 < CAP, main, pltpu.roll(tail, 6 - 2 * k, 1)))
            return 0

        lax.fori_loop(0, 4, step, 0)

    def put_send(d):
        def put(k, m, v):
            ps.at[d - 1, k].reshape(512, T)[pl.ds(pl.multiple_of(m * 128, 128), 128), :] = v.reshape(
                128, T
            ).astype(BF)

        return put

    def put_own(k, m, v):
        own[k, pl.ds(pl.multiple_of(m * 128, 128), 128), :] = v.reshape(128, T)

    lo = pl.ds(0, 32)
    hi = pl.ds(32, 32)
    packed(2, put_send(2))
    remote(ps.at[1, :, lo], hl, rs_send, rs_recv.at[0], right)
    remote(ps.at[1, :, hi], hr, rs_send, rs_recv.at[1], left)
    packed(3, put_send(3))
    remote(ps.at[2, :, hi], nl.at[:, hi], rs_send, rs_recv.at[2], right)
    packed(1, put_send(1))
    remote(ps.at[0, :, lo], nr.at[:, lo], rs_send, rs_recv.at[3], left)

    def merge(n, a, b):
        for k in range(3):
            mrg[n, k] = (a[k].astype(F32) + b[k].astype(F32)).astype(BF)

    wait(hl, rs_recv.at[0])
    merge(0, ps.at[2, :, lo], hl)
    remote(mrg.at[0], nl.at[:, lo], rs_send, rs_recv.at[4], right)
    wait(hr, rs_recv.at[1])
    merge(1, ps.at[0, :, hi], hr)
    remote(mrg.at[1], nr.at[:, hi], rs_send, rs_recv.at[5], left)
    packed(0, put_own)

    def scan(b, out):
        def at(i):
            return (
                lax.rem(z + NZ - i // PLANE, NZ) * PLANE
                + lax.rem(x + NX - lax.rem(i // NC, NX), NX) * NC
                + lax.rem(c + lax.rem(i, NC), NC)
            )

        def step(n, carry):
            s, t = carry
            jf = at(n)
            jb = at(NSP - 1 - n)
            low[jf] = s
            s = s * frecv[jf] + b[jf].astype(F32)
            high[jb] = t
            t = t * frecv[jb] + b[jb].astype(F32)
            return s, t

        zero = jnp.zeros((16, T), F32)
        lax.fori_loop(0, NSP, step, (zero, zero))

        def join(n, _):
            pos = pl.ds(n * 8, 8)
            out[pos] = jnp.where(iota((8, 16, T), 2) < 64, low[pos], high[pos]).astype(BF)
            return 0

        lax.fori_loop(0, 8, join, 0)

    def states_back(out, dst, n):
        def go(dz, p):
            zz, xx, cc = behind(dz, p)
            j = dz * PLANE + p
            remote(out.at[j], dst.at[me], st_send.at[n], st_recv.at[n], (zz, xx, cc, y))

        local(out.at[0], dst.at[me], self_sem.at[1 + n])
        to_all(go)

    def got_states(ref, n):
        wait(ref.at[pl.ds(1, NSP - 1)], st_recv.at[n])
        wait(ref.at[0], self_sem.at[1 + n])

    wait(frecv.at[pl.ds(1, NSP - 1)], st_recv.at[4])
    wait(frecv.at[0], self_sem.at[5])
    got_states(stw, 0)
    scan(stw, outw)

    wait(nl.at[:, hi], rs_recv.at[2])
    wait(nr.at[:, lo], rs_recv.at[3])
    wait(nl.at[:, lo], rs_recv.at[4])
    wait(nr.at[:, hi], rs_recv.at[5])
    for k in range(3):
        ret[k] = (
            own[k].reshape(64, 8, T) + nl[k].astype(F32) + nr[k].astype(F32)
        ).astype(BF)

    def send_back(dz, p):
        j = dz * PLANE + p
        remote(ret.at[:, j], rr.at[:, j], ret_send, ret_recv, behind(dz, p) + (y,))

    local(ret.at[:, 0], rr.at[:, 0], self_sem.at[6])
    to_all(send_back)
    states_back(outw, wsw, 1)

    def weight_grad(n, _):
        cols = pl.ds(pl.multiple_of(n * 256, 256), 256)
        src = pl.multiple_of(lax.rem(y + NY - n // 2, NY) * 512 + lax.rem(n, 2) * 256, 256)
        ow_gu[pl.ds(src, 256), :] = dot(xm[:, cols], gud[...], 0, 0).astype(BF)
        ow_d[:, pl.ds(src, 256)] = dot(hid[...], cm[:, cols], 0, 0).astype(BF)
        return 0

    lax.fori_loop(0, 8, weight_grad, 0)
    local(ow_gu.at[:, pl.ds(0, 256)], gg_o.at[0], o_sem.at[0])
    local(ow_gu.at[:, pl.ds(256, 256)], ug_o.at[0], o_sem.at[1])
    local(ow_d, dg_o.at[0], o_sem.at[2])

    common_t = dot(sw[...], sr[...], 1, 1)
    for h in range(HEADS):
        lst[h] = (lker[h] * common_t).astype(BF)

    wait(rr.at[:, pl.ds(1, NSP - 1)], ret_recv)
    wait(rr.at[:, 0], self_sem.at[6])
    tail = None
    for k in range(3):
        both = jnp.concatenate([comb[0], comb[1 + k]], axis=0)
        v = dot(both, rr.at[k].reshape(512, T)[...])
        lg[0, :, 128 * k : 128 * k + 128] = (
            cot[:, 128 * k : 128 * k + 128].astype(F32) + v[:T]
        ).astype(BF)
        tail = v[T:] if k == 0 else tail + v[T:]
    lg[0, :, 384:512] = (cot[:, 384:512].astype(F32) + tail).astype(BF)
    remote(lg.at[0], lg.at[1], lg_send, lg_recv.at[0], right)
    remote(lg.at[0], lg.at[3], lg_send, lg_recv.at[1], left)
    loaded(10)

    def out_part(d):
        v = dot(lg[d], pw[pl.ds(rows_of(d), 512), :])
        if d == 0:
            od[...] = v
        else:
            od[...] += v

    def transposed(d):
        for q in range(4):
            blkt = lg[d, :, 128 * q : 128 * q + 128].astype(F32).T.astype(BF)
            zz = lax.rem(y + NY - d, NY) * 2 + q // 2
            lt[zz, pl.ds(4 * (q % 2), 4)] = blkt.reshape(4, 32, T)

    out_part(0)
    wait(lg.at[1], lg_recv.at[0])
    remote(lg.at[1, pl.ds(0, 64)], lg.at[2, pl.ds(0, 64)], lg_send, lg_recv.at[2], right)
    wait(lg.at[3], lg_recv.at[1])
    remote(lg.at[3, pl.ds(64, 64)], lg.at[2, pl.ds(64, 64)], lg_send, lg_recv.at[3], left)
    out_part(1)
    out_part(3)
    transposed(0)
    transposed(1)
    transposed(3)
    wait(lg.at[2, pl.ds(0, 64)], lg_recv.at[2])
    wait(lg.at[2, pl.ds(64, 64)], lg_recv.at[3])
    out_part(2)
    odf = od[...].astype(BF).astype(F32)
    ogf = og[...].astype(F32)
    sig = jax.nn.sigmoid(ogf)
    delta = odf * (ogf * sig)
    od[...] = delta
    dl[...] = delta.astype(BF)

    sides(lambda k: od[:, 128 * k : 128 * k + 128], dfs, dfi)
    srt = sr[...].astype(F32).T.astype(BF)
    states(srt, dfs, sstr)
    send_state(sstr, strd, 2)
    transposed(2)
    for p in range(1, PLANE):
        zz, xx, cc = ahead(0, p)
        remote(
            lt.at[:, xx * NC + cc], rtm.at[:, :, pl.ds(T * p, T)], rt_send, rt_recv, (zz, xx, cc, y)
        )
    local(lt.at[:, plane], rtm.at[:, :, pl.ds(0, T)], self_sem.at[7])
    ow_o[...] = (odf * ms[...].astype(F32) * (sig * (1.0 + ogf * (1.0 - sig)))).astype(BF)
    local(ow_o, og_o, o_sem.at[7])

    wsum = None
    for h in range(HEADS):
        cols = slice(128 * (h // 2), 128 * (h // 2) + 128)
        mine = half if h % 2 == 0 else ~half
        dm = jnp.where(mine, od[:, cols], 0.0).astype(BF)
        part = lker[h] * dot(dm, hv[:, cols], 1, 1)
        wsum = part if h == 0 else wsum + part
    rgrad = dot(wsum.astype(BF), sw[...])
    wgrad = dot(wsum.T.astype(BF), sr[...])
    for k in range(HEADS // 2):
        cols = slice(128 * k, 128 * k + 128)
        a = dot(lst[2 * k], dl[:, cols])
        b = dot(lst[2 * k + 1], dl[:, cols])
        vint[:, cols] = jnp.where(half, a, b)
    got_states(wsw, 1)
    for h in range(HEADS):
        rgrad = rgrad + dot(dfi[h], wsw[pl.ds(8 * h, 8)].reshape(T, T), 1, 1)
    ow_r[...] = rgrad.astype(BF)
    local(ow_r, rg_o, o_sem.at[6])

    got_states(strd, 2)
    scan(strd, outr)
    states_back(outr, wsr, 3)

    wait(ga.at[pl.ds(1, PLANE - 1)], ga_recv)
    wait(rtm.at[:, :, pl.ds(T, T * (PLANE - 1))], rt_recv)
    wait(rtm.at[:, :, pl.ds(0, T)], self_sem.at[7])
    pg = dot(rtm[...].reshape(256, 1024), ga[...].reshape(1024, W))
    pgown[...] = pg.reshape(8, 32, W)
    pgs[...] = pg.reshape(8, 32, W).astype(BF)
    for dz in (1, 7, 2, 6, 3, 5, 4):
        zz = lax.rem(z + dz, NZ)
        remote(pgs.at[zz], zr.at[dz], z_send, z_recv, (zz, x, c, y))

    got_states(wsr, 3)
    for k in range(HEADS // 2):
        cols = slice(128 * k, 128 * k + 128)
        u = []
        for h in (2 * k, 2 * k + 1):
            state = wsr[pl.ds(8 * h, 8)].reshape(T, T)
            p = dot(sw[...], state) * fts[h]
            u.append(p + pltpu.roll(p, 64, 1))
            wgrad = wgrad + dot(vfi[h], state, 1, 1)
        ow_v[:, cols] = (vint[:, cols] + jnp.where(half, u[0], u[1])).astype(BF)
    ow_w[...] = wgrad.astype(BF)
    local(ow_v, vg_o, o_sem.at[4])
    local(ow_w, wg_o, o_sem.at[5])

    wait(zr.at[pl.ds(1, NZ - 1)], z_recv)
    total = pgown[z]
    for dz in range(1, NZ):
        total = total + zr[dz].astype(F32)
    ow_p[...] = total
    local(ow_p, pg_o, o_sem.at[3])

    wait(sx.at[:, pl.ds(1, NSP - 1)], d_send)
    wait(gy.at[pl.ds(1, 3)], y_send)
    wait(ps, rs_send)
    wait(ret.at[:, pl.ds(1, NSP - 1)], ret_send)
    wait(lg.at[pl.ds(0, 3)], lg_send)
    for n in range(4):
        wait(stw.at[pl.ds(1, NSP - 1)], st_send.at[n])
    wait(frecv.at[pl.ds(1, NSP - 1)], st_send.at[4])
    wait(ga.at[pl.ds(1, PLANE - 1)], ga_send)
    wait(rtm.at[:, :, pl.ds(T, T * (PLANE - 1))], rt_send)
    wait(zr.at[pl.ds(1, NZ - 1)], z_send)
    stores = (
        (ow_gu.at[:, pl.ds(0, 256)], gg_o.at[0]), (ow_gu.at[:, pl.ds(256, 256)], ug_o.at[0]),
        (ow_d, dg_o.at[0]), (ow_p, pg_o), (ow_v, vg_o), (ow_w, wg_o), (ow_r, rg_o), (ow_o, og_o),
    )
    for n, (a, b) in enumerate(stores):
        pltpu.make_async_copy(a, b, o_sem.at[n]).wait()


def bf(*shape):
    return pltpu.VMEM(shape, BF)


def fl(*shape):
    return pltpu.VMEM(shape, F32)


def sem(n):
    return pltpu.SemaphoreType.DMA((n,))


SCRATCH = (
    bf(T, W),
    bf(T, W),
    bf(2048, 512),
    bf(256, 2048),
    bf(T, W),
    bf(T, W),
    bf(T, W),
    bf(2048, 512),
    bf(T, T),
    bf(T, T),
    bf(6, 64, 8, T),
    bf(4, 6, 64, 8, T),
    bf(512, 2048),
    bf(512, 2048),
    fl(512, 512),
    fl(512, 256),
    bf(512, 512),
    bf(512, 256),
    bf(3, 3, 64, 8, T),
    fl(3, 512, T),
    bf(3, 32, 8, T),
    bf(3, 32, 8, T),
    bf(2, 3, 32, 8, T),
    bf(3, 64, 8, T),
    bf(3, 64, 8, T),
    bf(3, 64, 8, T),
    bf(3, 64, 8, T),
    bf(4, T, 512),
    bf(4, T, W),
    fl(T, W),
    bf(T, W),
    bf(64, 16, T),
    bf(64, 16, T),
    bf(64, 16, T),
    bf(64, 16, T),
    fl(64, 16, T),
    fl(64, 16, T),
    bf(64, 16, T),
    bf(64, 16, T),
    bf(64, 16, T),
    bf(64, 16, T),
    fl(8, 1, T),
    fl(64, 1, T),
    bf(8, T, T),
    bf(8, T, T),
    bf(8, T, T),
    bf(8, T, T),
    fl(8, T, T),
    bf(8, T, T),
    fl(8, T, T),
    fl(T, W),
    bf(8, 8, 32, T),
    bf(8, 32, 1024),
    bf(8, T, W),
    bf(8, 32, W),
    bf(8, 32, W),
    fl(8, 32, W),
    bf(2048, 512),
    bf(256, 2048),
    fl(32, W),
    bf(T, W),
    bf(T, T),
    bf(T, T),
    bf(T, W),
    sem(11),
    sem(8),
    sem(9),
    pltpu.SemaphoreType.DMA,
    sem(8),
    pltpu.SemaphoreType.DMA,
    sem(8),
    sem(8),
    sem(8),
    pltpu.SemaphoreType.DMA,
    sem(6),
    pltpu.SemaphoreType.DMA,
    pltpu.SemaphoreType.DMA,
    pltpu.SemaphoreType.DMA,
    sem(4),
    sem(5),
    sem(5),
    pltpu.SemaphoreType.DMA,
    pltpu.SemaphoreType.DMA,
    pltpu.SemaphoreType.DMA,
    pltpu.SemaphoreType.DMA,
    pltpu.SemaphoreType.DMA,
    pltpu.SemaphoreType.DMA,
)


def on_device(
    layer_input, cotangent, routes, route_weight, gate_weight, up_weight, down_weight, heads_value,
    output_gate, mixer_saved, proj_weight, state_write, state_read, decay_rate,
):
    hbm = pl.BlockSpec(memory_space=pl.ANY)
    vmem = pl.BlockSpec(memory_space=pltpu.VMEM)
    shape = jax.ShapeDtypeStruct
    return pl.pallas_call(
        body,
        name="layer_backward",
        out_shape=(
            shape((1, 2048, 256), BF), shape((1, 2048, 256), BF), shape((1, 256, 2048), BF),
            shape((32, W), F32), shape((T, W), BF), shape((T, T), BF), shape((T, T), BF),
            shape((T, W), BF),
        ),
        in_specs=[hbm, hbm, vmem, vmem] + [hbm] * 9 + [vmem],
        out_specs=tuple([hbm] * 8),
        scratch_shapes=SCRATCH,
        compiler_params=pltpu.CompilerParams(
            collective_id=0, has_side_effects=True, vmem_limit_bytes=60 * 1024 * 1024
        ),
    )(
        layer_input, cotangent, routes.T, route_weight.T, gate_weight, up_weight, down_weight,
        heads_value, output_gate, mixer_saved, proj_weight, state_write, state_read, decay_rate.T,
    )


def solution(mesh):
    split = Mesh(mesh.devices.reshape(NZ, NX, NC, mesh.shape["tp"]), SP + ("tp",))
    rows, cut = P(SP, None), P(SP, "tp")
    return jax.shard_map(
        on_device,
        mesh=split,
        in_specs=(
            cut, cut, rows, rows, P(SP, None, "tp"), P(SP, None, "tp"), P(SP, "tp", None), cut, cut,
            cut, P(None, "tp"), cut, cut, cut,
        ),
        out_specs=(
            P(SP, None, "tp"), P(SP, None, "tp"), P(SP, "tp", None), cut, cut, cut, cut, cut,
        ),
        check_vma=False,
    )
```

time: 399 us -> 125 us (0.31)
  blocking collectives: 219 us -> 0 us
  Pallas kernels: 0 us -> 116 us
  waiting for transfers between devices: 67.5 us -> 0 us
  matrix products: 30.6 us -> 0 us
  other arithmetic: 24.9 us -> 0 us
  starting transfers between devices: 16.9 us -> 0 us
  local copies, waits for them, and re-layouts: 23.9 us -> 7.55 us
  between operations: 14.9 us -> 0.69 us
    all_gather x13 -> x0, blocking collectives: 166 us -> none  [the longest x12 154 us: prefix_by_axis(): lax.all_gather(part.astype(kind), axis)]
    pallas_call x0 -> x1, Pallas kernels: none -> 116 us  [on_device(): pl.pallas_call(body, name='layer_backward', out_shape=(shape((1, 2048, 25...]
    all_to_all x2 -> x0, blocking collectives: 52.5 us -> none  [the longest x1 29.4 us: on_device(): lax.all_to_all(fill_slots(layer_input), SP, split_axis=0, concat_axis=0,...]
    all_gather x6 -> x0, waiting for transfers between devices: 40.4 us -> none  [the longest x1 23.2 us: on_device(): lax.all_gather(part_cotangent, 'tp', axis=1, tiled=True)]
    dot_general x20 -> x0, matrix products: 30.6 us -> none  [the longest x1 3.28 us: on_device(): lax.dot_general(expert_input, up_delta, contract_first, preferred_element...]
    all_to_all x2 -> x0, starting transfers between devices: 16.6 us -> none  [the longest x1 10.4 us: on_device(): lax.all_to_all(returned, SP, split_axis=0, concat_axis=0, tiled=True)]
    all_to_all x2 -> x0, waiting for transfers between devices: 13.6 us -> none  [the longest x1 13.6 us: on_device(): lax.all_to_all(returned, SP, split_axis=0, concat_axis=0, tiled=True)]
    reduce_scatter x1 -> x0, waiting for transfers between devices: 12.9 us -> none  [on_device(): lax.psum_scatter(rounded.astype(jnp.bfloat16), 'tp', scatter_dimension=1,...]
  transfers between devices with their start and end apart: 9 -> 0, of which waited for: 4 -> 0; matrix products, arithmetic and copies ran while one was open for 13% -> 0% of each run, Pallas kernels for 0% -> 0%
where the time goes in v1:
time: 125 us; the launch traced here: 124 us
  Pallas kernels  116 us (93%)
  local copies, waits for them, and re-layouts  7.55 us (6%)
    pallas_call x1, Pallas kernels, on_device(): pl.pallas_call(body, name='layer_backward', out_shape=(shape((1, 2048, 25...  116 us
    unnamed x22, local copies, waits for them, and re-layouts  7.55 us

profile of v1, /device:TPU:24, one launch (start us, length us, event | category | flops | bytes accessed | tf_op | source)
XLA Modules:
  0.0 123.9 jit_solution(4674338845530353459)
XLA Ops:
  0.6 115.7 %layer_backward.1 = (bf16[1,2048,256]{2,1,0:T(8,128)(2,1)}, bf16[1,2048,256]{2,1,0:T(8,128)(2,1)}, bf16[1,256,2048]{2,1,0:T(8,128)(2,1)}, f32[32,512]{1,0:T(8,12...) custom-call(bf16[128,512]{1,0:T(8,128)(2,1)} %li_h.1, ...), custom_call_target="tpu_custom_call" | custom-call | tf_op jit(solution)/shard_map/layer_backward/pallas_call | solution.py:699
  116.4 0.0 copy-start.1
  116.4 0.0 copy-start
  116.4 2.4 %copy.30 = bf16[1,2048,256]{2,1,0:T(8,128)(2,1)} copy(bf16[1,2048,256]{2,1,0:T(8,128)(2,1)} %get-tuple-element.16) | data formatting | bytes 2097152
  118.8 0.0 copy-done.1
  118.8 0.0 copy-start.4
  118.8 0.0 copy-start.3
  118.8 0.0 copy-start.6
  118.8 0.0 copy-start.5
  118.8 0.0 copy-start.2
  118.8 1.0 copy.31
  119.8 0.0 copy-done
  119.8 1.0 copy.32
  120.8 0.0 copy-done.4
  120.8 0.6 copy.33
  121.4 0.0 copy-done.3
  121.4 0.7 copy.34
  122.1 0.0 copy-done.6
  122.1 0.6 copy.35
  122.7 0.0 copy-done.5
  122.7 0.6 copy.36
  123.3 0.0 copy-done.2
  123.3 0.7 copy.37
Async XLA Ops:
  116.4 2.4 %copy-start.1 = (bf16[1,2048,256]{2,1,0:T(8,128)(2,1)S(1)}, bf16[1,2048,256]{2,1,0:T(8,128)(2,1)}, u32[]{:S(2)}) copy-start(bf16[1,2048,256]{2,1,0:T(8,128)(2,1)} %get-tuple-element.17) | copy-start | bytes 3145732
  116.4 3.4 %copy-start = (bf16[1,256,2048]{2,1,0:T(8,128)(2,1)S(1)}, bf16[1,256,2048]{2,1,0:T(8,128)(2,1)}, u32[]{:S(2)}) copy-start(bf16[1,256,2048]{2,1,0:T(8,128)(2,1)} %get-tuple-element.18) | copy-start | bytes 3145732
  118.8 2.0 %copy-start.4 = (f32[32,512]{1,0:T(8,128)S(1)}, f32[32,512]{1,0:T(8,128)}, u32[]{:S(2)}) copy-start(f32[32,512]{1,0:T(8,128)} %get-tuple-element.19) | copy-start | bytes 196612
  118.8 2.6 %copy-start.3 = (bf16[128,512]{1,0:T(8,128)(2,1)S(1)}, bf16[128,512]{1,0:T(8,128)(2,1)}, u32[]{:S(2)}) copy-start(bf16[128,512]{1,0:T(8,128)(2,1)} %get-tuple-element.20) | copy-start | bytes 393220
  118.8 3.3 %copy-start.6 = (bf16[128,128]{1,0:T(8,128)(2,1)S(1)}, bf16[128,128]{1,0:T(8,128)(2,1)}, u32[]{:S(2)}) copy-start(bf16[128,128]{1,0:T(8,128)(2,1)} %get-tuple-element.21) | copy-start | bytes 98308
  118.8 3.9 %copy-start.5 = (bf16[128,128]{1,0:T(8,128)(2,1)S(1)}, bf16[128,128]{1,0:T(8,128)(2,1)}, u32[]{:S(2)}) copy-start(bf16[128,128]{1,0:T(8,128)(2,1)} %get-tuple-element.22) | copy-start | bytes 98308
  118.8 4.5 %copy-start.2 = (bf16[128,512]{1,0:T(8,128)(2,1)S(1)}, bf16[128,512]{1,0:T(8,128)(2,1)}, u32[]{:S(2)}) copy-start(bf16[128,512]{1,0:T(8,128)(2,1)} %get-tuple-element.23) | copy-start | bytes 393220

commit v2 on v1

--- a/solution.py
+++ b/solution.py
@@ -17,6 +17,10 @@
 BF = jnp.bfloat16
 F32 = jnp.float32
 ORDER = (0, 1, 7, 2, 6, 3, 5, 4)
+GROUPS = 2
+GC = NZ // GROUPS
+GJ = GC * PLANE
+GR = GJ * 8
 MESH_ID = pl.DeviceIdType.MESH
 HIGH = lax.Precision.HIGHEST
 
@@ -40,7 +44,7 @@
         li, cot, gu, dw, hv, og, ms, pw, sw, sr, sx, gy, xm, cm, acc_gu, acc_h, gud, hid, ps,
         own, hl, hr, mrg, nl, nr, ret, rr, comb, lg, od, dl, sstw, sstr, stw, strd, low, high,
         outw, outr, wsw, wsr, fsend, frecv, vfs, vfi, dfs, dfi, fts, lst, lker, vint, lt, rtm,
-        ga, pgs, zr, pgown, ow_gu, ow_d, ow_p, ow_v, ow_w, ow_r, ow_o, ld_sem, o_sem, self_sem,
+        ga, pgs, zr, pgown, ld_sem, self_sem,
         d_send, d_recv, y_send, yl_recv, yr_recv, yo_recv, rs_send, rs_recv, ret_send, ret_recv,
         lg_send, lg_recv, st_send, st_recv, ga_send, ga_recv, rt_send, rt_recv, z_send, z_recv,
 
@@ -82,18 +86,26 @@
     def wait(ref, sem):
         pltpu.make_async_copy(ref, ref, sem).wait()
 
-    def to_all(send):
-        for p in range(1, PLANE):
-            send(0, p)
+    def dz_of(n):
+        odd = lax.rem(n, 2)
+        return lax.rem(odd * ((n + 1) // 2) + (1 - odd) * (NZ - n // 2), NZ)
+
+    def n_of(dz):
+        far = dz // 5
+        return (1 - far) * (2 * dz - 1) + far * (16 - 2 * dz) + (NZ - dz) // NZ
+
+    def to_all(send, first=0, last=NZ):
+        if first == 0:
+            for p in range(1, PLANE):
+                send(0, 0, p)
 
         def step(n, _):
-            odd = lax.rem(n, 2)
-            dz = odd * ((n + 1) // 2) + (1 - odd) * (NZ - n // 2)
+            dz = dz_of(n)
             for p in range(PLANE):
-                send(dz, p)
+                send(n, dz, p)
             return 0
 
-        lax.fori_loop(1, NZ, step, 0)
+        lax.fori_loop(max(first, 1), last, step, 0)
 
     loads = (
         (li_h, li), (cot_h, cot), (hv_h, hv), (sw_h, sw), (sr_h, sr), (og_h, og), (ms_h, ms),
@@ -111,7 +123,7 @@
     def greet(dev):
         pl.semaphore_signal(bar, inc=1, device_id=dev, device_id_type=MESH_ID)
 
-    to_all(lambda dz, p: greet(ahead(dz, p) + (y,)))
+    to_all(lambda n, dz, p: greet(ahead(dz, p) + (y,)))
     greet(right)
     greet(left)
     greet(opposite)
@@ -120,7 +132,7 @@
     r8 = lax.rem(ci, 8)
     blk = ci // 8
     e = (
-        lax.rem(z + blk // PLANE, NZ) * PLANE
+        lax.rem(z + dz_of(blk // PLANE), NZ) * PLANE
         + lax.rem(x + lax.rem(blk // NC, NX), NX) * NC
         + lax.rem(c + lax.rem(blk, NC), NC)
     )
@@ -158,15 +170,6 @@
     for k in range(3):
         comb[1 + k] = extra[k].T.astype(BF)
 
-    pl.semaphore_wait(bar, NSP - 1 + 3)
-
-    def send_x(dz, p):
-        j = dz * PLANE + p
-        remote(sx.at[:, j], gy.at[0, :, j], d_send, d_recv.at[dz], ahead(dz, p) + (y,))
-
-    local(sx.at[:, 0], gy.at[0, :, 0], self_sem.at[0])
-    to_all(send_x)
-
     loaded(2)
     loaded(3)
     loaded(4)
@@ -210,171 +213,234 @@
     states(swt, vfs, sstw)
 
     def send_state(src, dst, n):
-        def go(dz, p):
+        def go(n_, dz, p):
             zz, xx, cc = ahead(dz, p)
-            j = dz * PLANE + p
+            j = n_ * PLANE + p
             remote(src.at[zz * PLANE + xx * NC + cc], dst.at[j], st_send.at[n], st_recv.at[n], (zz, xx, cc, y))
 
         local(src.at[me], dst.at[0], self_sem.at[1 + n])
         to_all(go)
 
-    def send_fade(dz, p):
+    def send_fade(n, dz, p):
         zz, xx, cc = ahead(dz, p)
-        j = dz * PLANE + p
+        j = n * PLANE + p
         remote(fsend.at[zz], frecv.at[j], st_send.at[4], st_recv.at[4], (zz, xx, cc, y))
-
-    local(fsend.at[z], frecv.at[0], self_sem.at[5])
-    to_all(send_fade)
-    send_state(sstw, stw, 0)
 
     loaded(5)
     loaded(6)
     ogf = og[...].astype(F32)
     sig = jax.nn.sigmoid(ogf)
     ga[0] = (ms[...].astype(F32) * (ogf * sig)).astype(BF)
+    pl.semaphore_wait(bar, NSP - 1 + 3)
+
+    def send_x(n, dz, p):
+        j = n * PLANE + p
+        remote(sx.at[:, j], gy.at[0, :, j], d_send, d_recv.at[n], ahead(dz, p) + (y,))
+
+    local(sx.at[:, 0], gy.at[0, :, 0], self_sem.at[0])
+    to_all(send_x)
+
+    local(fsend.at[z], frecv.at[0], self_sem.at[5])
+    to_all(send_fade)
+    send_state(sstw, stw, 0)
+
     for p in range(1, PLANE):
         remote(ga.at[0], ga.at[p], ga_send, ga_recv, ahead(0, p) + (y,))
 
-    def chunk(d, dz):
-        return gy.at[d, :, pl.ds(PLANE * dz, PLANE)]
+    def chunk(d, n):
+        return gy.at[d, :, pl.ds(PLANE * n, PLANE)]
 
     def forward(n):
-        dz = ORDER[n]
         if n % 2 == 0:
-            wait(chunk(1, dz), yl_recv.at[n])
-            remote(chunk(1, dz), chunk(2, dz), y_send, yo_recv.at[n], right)
+            wait(chunk(1, n), yl_recv.at[n])
+            remote(chunk(1, n), chunk(2, n), y_send, yo_recv.at[n], right)
         else:
-            wait(chunk(3, dz), yr_recv.at[n])
-            remote(chunk(3, dz), chunk(2, dz), y_send, yo_recv.at[n], left)
-
-    for n, dz in enumerate(ORDER):
-        if dz == 0:
+            wait(chunk(3, n), yr_recv.at[n])
+            remote(chunk(3, n), chunk(2, n), y_send, yo_recv.at[n], left)
+
+    def arrived(n):
+        if n == 0:
             wait(gy.at[0, :, pl.ds(1, PLANE - 1)], d_recv.at[0])
             wait(gy.at[0, :, 0], self_sem.at[0])
         else:
-            wait(chunk(0, dz), d_recv.at[dz])
-        remote(chunk(0, dz), chunk(1, dz), y_send, yl_recv.at[n], right)
-        remote(chunk(0, dz), chunk(3, dz), y_send, yr_recv.at[n], left)
-        if n >= 1:
-            forward(n - 1)
-
-    r3 = iota((64, 8, T), 1)
-
-    def assemble(d, first, dst):
+            wait(chunk(0, n), d_recv.at[n])
+        remote(chunk(0, n), chunk(1, n), y_send, yl_recv.at[n], right)
+        remote(chunk(0, n), chunk(3, n), y_send, yr_recv.at[n], left)
+
+    def slices(g, d):
+        for n in range(GC * g, GC * g + GC):
+            if d == 1 and n % 2 == 1:
+                wait(chunk(1, n), yl_recv.at[n])
+            if d == 3 and n % 2 == 0:
+                wait(chunk(3, n), yr_recv.at[n])
+            if d == 2:
+                wait(chunk(2, n), yo_recv.at[n])
+
+    r3 = iota((GJ, 8, T), 1)
+
+    def assemble(g, d, first, dst):
         last = None
+        rows = pl.ds(GR * g, GR)
+        js = pl.ds(GJ * g, GJ)
         for k in range(3):
-            dst[:, pl.ds(512 * d + 128 * k, 128)] = gy.at[d, first + k].reshape(512, T)[...]
-            moved = pltpu.roll(gy[d, first + k].astype(F32), 2 * k + 2, 1)
+            dst[rows, pl.ds(512 * d + 128 * k, 128)] = gy.at[d, first + k].reshape(512, T)[rows, :]
+            moved = pltpu.roll(gy[d, first + k, js].astype(F32), 2 * k + 2, 1)
             last = moved if k == 0 else jnp.where(r3 // 2 == k, moved, last)
-        dst[:, pl.ds(512 * d + 384, 128)] = last.reshape(512, T).astype(BF)
+        dst[rows, pl.ds(512 * d + 384, 128)] = last.reshape(GR, T).astype(BF)
 
     def rows_of(d):
         return pl.multiple_of(lax.rem(y + NY - d, NY) * 512, 512)
 
-    def expert_in(d, start):
-        assemble(d, 0, xm)
-        assemble(d, 3, cm)
+    def expert_in(g, d):
+        slices(g, d)
+        assemble(g, d, 0, xm)
+        assemble(g, d, 3, cm)
         off = rows_of(d)
+        rows = pl.ds(GR * g, GR)
+        a = dot(xm[rows, pl.ds(512 * d, 512)], gu[pl.ds(off, 512), :])
+        b = dot(cm[rows, pl.ds(512 * d, 512)], dw[:, pl.ds(off, 512)], 1, 1)
+        if d == 0:
+            acc_gu[rows, :] = a
+            acc_h[rows, :] = b
+        else:
+            acc_gu[rows, :] += a
+            acc_h[rows, :] += b
+
+    def activations(g):
+        def middle(m, _):
+            rows = pl.ds(pl.multiple_of(GR * g + m * 64, 64), 64)
+            keep = lax.rem(iota((64, 256), 0), 8) < CAP
+            gt = acc_gu[rows, pl.ds(0, 256)]
+            u = acc_gu[rows, pl.ds(256, 256)]
+            hg = acc_h[rows, :]
+            s = jax.nn.sigmoid(gt)
+            act = gt * s
+            slope = s * (1.0 + gt * (1.0 - s))
+            hid[rows, :] = jnp.where(keep, act * u, 0.0).astype(BF)
+            gud[rows, pl.ds(0, 256)] = jnp.where(keep, hg * u * slope, 0.0).astype(BF)
+            gud[rows, pl.ds(256, 256)] = jnp.where(keep, hg * act, 0.0).astype(BF)
+            return 0
+
+        lax.fori_loop(0, GR // 64, middle, 0)
+
+    def packed(g, d, put):
+        off = rows_of(d)
 
         def step(m, _):
-            rows = pl.ds(pl.multiple_of(m * 256, 256), 256)
-            a = dot(xm[rows, pl.ds(512 * d, 512)], gu[pl.ds(off, 512), :])
-            b = dot(cm[rows, pl.ds(512 * d, 512)], dw[:, pl.ds(off, 512)], 1, 1)
-            if start:
-                acc_gu[rows, :] = a
-                acc_h[rows, :] = b
-            else:
-                acc_gu[rows, :] += a
-                acc_h[rows, :] += b
-            return 0
-
-        lax.fori_loop(0, 2, step, 0)
-
-    loaded(7)
-    loaded(8)
-    loaded(9)
-    forward(7)
-    expert_in(0, True)
-    for n in range(8):
-        if n % 2 == 1:
-            wait(chunk(1, ORDER[n]), yl_recv.at[n])
-    expert_in(1, False)
-    for n in range(8):
-        if n % 2 == 0:
-            wait(chunk(3, ORDER[n]), yr_recv.at[n])
-    expert_in(3, False)
-    for n in range(8):
-        wait(chunk(2, ORDER[n]), yo_recv.at[n])
-    expert_in(2, False)
-
-    def middle(m, _):
-        rows = pl.ds(pl.multiple_of(m * 64, 64), 64)
-        keep = lax.rem(iota((64, 256), 0), 8) < CAP
-        g = acc_gu[rows, pl.ds(0, 256)]
-        u = acc_gu[rows, pl.ds(256, 256)]
-        hg = acc_h[rows, :]
-        s = jax.nn.sigmoid(g)
-        act = g * s
-        slope = s * (1.0 + g * (1.0 - s))
-        hid[rows, :] = jnp.where(keep, act * u, 0.0).astype(BF)
-        gud[rows, pl.ds(0, 256)] = jnp.where(keep, hg * u * slope, 0.0).astype(BF)
-        gud[rows, pl.ds(256, 256)] = jnp.where(keep, hg * act, 0.0).astype(BF)
-        return 0
-
-    lax.fori_loop(0, 8, middle, 0)
-
-    def packed(d, put):
-        off = rows_of(d)
-
-        def step(m, _):
-            rows = pl.ds(pl.multiple_of(m * 128, 128), 128)
+            rows = pl.ds(pl.multiple_of(GR * g + m * 128, 128), 128)
             a = dot(gud[rows, :], gu[pl.ds(off, 512), :], 1, 1)
             tail = a[:, 384:512].reshape(16, 8, T)
             rr3 = iota((16, 8, T), 1)
             for k in range(3):
                 main = a[:, 128 * k : 128 * k + 128].reshape(16, 8, T)
-                put(k, m, jnp.where(rr3 < CAP, main, pltpu.roll(tail, 6 - 2 * k, 1)))
+                put(k, rows, jnp.where(rr3 < CAP, main, pltpu.roll(tail, 6 - 2 * k, 1)))
             return 0
 
-        lax.fori_loop(0, 4, step, 0)
+        lax.fori_loop(0, GR // 128, step, 0)
 
     def put_send(d):
-        def put(k, m, v):
-            ps.at[d - 1, k].reshape(512, T)[pl.ds(pl.multiple_of(m * 128, 128), 128), :] = v.reshape(
-                128, T
+        def put(k, rows, v):
+            ps.at[d - 1, k].reshape(512, T)[rows, :] = v.reshape(128, T).astype(BF)
+
+        return put
+
+    def put_own(k, rows, v):
+        own[k, rows, :] = v.reshape(128, T)
+
+    HJ = GJ // 2
+
+    def lo(g):
+        return pl.ds(GJ * g, HJ)
+
+    def hi(g):
+        return pl.ds(GJ * g + HJ, HJ)
+
+    def far_partials(g):
+        packed(g, 2, put_send(2))
+        remote(ps.at[1, :, lo(g)], hl.at[g], rs_send, rs_recv.at[6 * g], right)
+        remote(ps.at[1, :, hi(g)], hr.at[g], rs_send, rs_recv.at[6 * g + 1], left)
+
+    def right_partials(g):
+        packed(g, 3, put_send(3))
+        remote(ps.at[2, :, hi(g)], nl.at[:, hi(g)], rs_send, rs_recv.at[6 * g + 2], right)
+
+    def left_partials(g):
+        packed(g, 1, put_send(1))
+        remote(ps.at[0, :, lo(g)], nr.at[:, lo(g)], rs_send, rs_recv.at[6 * g + 3], left)
+
+    def merge(g):
+        wait(hl.at[g], rs_recv.at[6 * g])
+        for k in range(3):
+            mrg[0, g, k] = (ps[2, k, lo(g)].astype(F32) + hl[g, k].astype(F32)).astype(BF)
+        remote(mrg.at[0, g], nl.at[:, lo(g)], rs_send, rs_recv.at[6 * g + 4], right)
+        wait(hr.at[g], rs_recv.at[6 * g + 1])
+        for k in range(3):
+            mrg[1, g, k] = (ps[0, k, hi(g)].astype(F32) + hr[g, k].astype(F32)).astype(BF)
+        remote(mrg.at[1, g], nr.at[:, hi(g)], rs_send, rs_recv.at[6 * g + 5], left)
+
+    def send_back(n, dz, p):
+        j = n * PLANE + p
+        remote(ret.at[:, j], rr.at[:, j], ret_send, ret_recv.at[n // GC], behind(dz, p) + (y,))
+
+    def give_back(g):
+        wait(nl.at[:, hi(g)], rs_recv.at[6 * g + 2])
+        wait(nr.at[:, lo(g)], rs_recv.at[6 * g + 3])
+        wait(nl.at[:, lo(g)], rs_recv.at[6 * g + 4])
+        wait(nr.at[:, hi(g)], rs_recv.at[6 * g + 5])
+        js = pl.ds(GJ * g, GJ)
+        for k in range(3):
+            ret[k, js] = (
+                own[k, pl.ds(GR * g, GR)].reshape(GJ, 8, T)
+                + nl[k, js].astype(F32)
+                + nr[k, js].astype(F32)
             ).astype(BF)
-
-        return put
-
-    def put_own(k, m, v):
-        own[k, pl.ds(pl.multiple_of(m * 128, 128), 128), :] = v.reshape(128, T)
-
-    lo = pl.ds(0, 32)
-    hi = pl.ds(32, 32)
-    packed(2, put_send(2))
-    remote(ps.at[1, :, lo], hl, rs_send, rs_recv.at[0], right)
-    remote(ps.at[1, :, hi], hr, rs_send, rs_recv.at[1], left)
-    packed(3, put_send(3))
-    remote(ps.at[2, :, hi], nl.at[:, hi], rs_send, rs_recv.at[2], right)
-    packed(1, put_send(1))
-    remote(ps.at[0, :, lo], nr.at[:, lo], rs_send, rs_recv.at[3], left)
-
-    def merge(n, a, b):
-        for k in range(3):
-            mrg[n, k] = (a[k].astype(F32) + b[k].astype(F32)).astype(BF)
-
-    wait(hl, rs_recv.at[0])
-    merge(0, ps.at[2, :, lo], hl)
-    remote(mrg.at[0], nl.at[:, lo], rs_send, rs_recv.at[4], right)
-    wait(hr, rs_recv.at[1])
-    merge(1, ps.at[0, :, hi], hr)
-    remote(mrg.at[1], nr.at[:, hi], rs_send, rs_recv.at[5], left)
-    packed(0, put_own)
+        if g == 0:
+            local(ret.at[:, 0], rr.at[:, 0], self_sem.at[6])
+        to_all(send_back, GC * g, GC * g + GC)
+
+    for n in range(4):
+        arrived(n)
+        if n >= 2:
+            forward(n - 2)
+    loaded(7)
+    loaded(8)
+    loaded(9)
+    arrived(4)
+    forward(2)
+    expert_in(0, 0)
+    arrived(5)
+    forward(3)
+    expert_in(0, 1)
+    arrived(6)
+    forward(4)
+    expert_in(0, 3)
+    arrived(7)
+    forward(5)
+    expert_in(0, 2)
+    forward(6)
+    activations(0)
+    forward(7)
+    far_partials(0)
+    right_partials(0)
+    left_partials(0)
+    expert_in(1, 0)
+    merge(0)
+    expert_in(1, 1)
+    packed(0, 0, put_own)
+    expert_in(1, 3)
+    expert_in(1, 2)
+    activations(1)
+    far_partials(1)
+    right_partials(1)
+    left_partials(1)
+    give_back(0)
+    merge(1)
+    packed(1, 0, put_own)
 
     def scan(b, out):
         def at(i):
             return (
-                lax.rem(z + NZ - i // PLANE, NZ) * PLANE
+                n_of(lax.rem(z + NZ - i // PLANE, NZ)) * PLANE
                 + lax.rem(x + NX - lax.rem(i // NC, NX), NX) * NC
                 + lax.rem(c + lax.rem(i, NC), NC)
             )
@@ -400,9 +466,9 @@
         lax.fori_loop(0, 8, join, 0)
 
     def states_back(out, dst, n):
-        def go(dz, p):
+        def go(n_, dz, p):
             zz, xx, cc = behind(dz, p)
-            j = dz * PLANE + p
+            j = n_ * PLANE + p
             remote(out.at[j], dst.at[me], st_send.at[n], st_recv.at[n], (zz, xx, cc, y))
 
         local(out.at[0], dst.at[me], self_sem.at[1 + n])
@@ -417,50 +483,44 @@
     got_states(stw, 0)
     scan(stw, outw)
 
-    wait(nl.at[:, hi], rs_recv.at[2])
-    wait(nr.at[:, lo], rs_recv.at[3])
-    wait(nl.at[:, lo], rs_recv.at[4])
-    wait(nr.at[:, hi], rs_recv.at[5])
-    for k in range(3):
-        ret[k] = (
-            own[k].reshape(64, 8, T) + nl[k].astype(F32) + nr[k].astype(F32)
-        ).astype(BF)
-
-    def send_back(dz, p):
-        j = dz * PLANE + p
-        remote(ret.at[:, j], rr.at[:, j], ret_send, ret_recv, behind(dz, p) + (y,))
-
-    local(ret.at[:, 0], rr.at[:, 0], self_sem.at[6])
-    to_all(send_back)
+    give_back(1)
     states_back(outw, wsw, 1)
 
     def weight_grad(n, _):
         cols = pl.ds(pl.multiple_of(n * 256, 256), 256)
         src = pl.multiple_of(lax.rem(y + NY - n // 2, NY) * 512 + lax.rem(n, 2) * 256, 256)
-        ow_gu[pl.ds(src, 256), :] = dot(xm[:, cols], gud[...], 0, 0).astype(BF)
-        ow_d[:, pl.ds(src, 256)] = dot(hid[...], cm[:, cols], 0, 0).astype(BF)
+        both = dot(xm[:, cols], gud[...], 0, 0).astype(BF)
+        gg_o[0, pl.ds(src, 256), :] = both[:, :256]
+        ug_o[0, pl.ds(src, 256), :] = both[:, 256:]
+        dg_o[0, :, pl.ds(src, 256)] = dot(hid[...], cm[:, cols], 0, 0).astype(BF)
         return 0
 
     lax.fori_loop(0, 8, weight_grad, 0)
-    local(ow_gu.at[:, pl.ds(0, 256)], gg_o.at[0], o_sem.at[0])
-    local(ow_gu.at[:, pl.ds(256, 256)], ug_o.at[0], o_sem.at[1])
-    local(ow_d, dg_o.at[0], o_sem.at[2])
-
     common_t = dot(sw[...], sr[...], 1, 1)
     for h in range(HEADS):
         lst[h] = (lker[h] * common_t).astype(BF)
 
-    wait(rr.at[:, pl.ds(1, NSP - 1)], ret_recv)
-    wait(rr.at[:, 0], self_sem.at[6])
-    tail = None
-    for k in range(3):
-        both = jnp.concatenate([comb[0], comb[1 + k]], axis=0)
-        v = dot(both, rr.at[k].reshape(512, T)[...])
+    moe = None
+    for g in range(GROUPS):
+        if g == 0:
+            wait(rr.at[:, pl.ds(1, GJ - 1)], ret_recv.at[0])
+            wait(rr.at[:, 0], self_sem.at[6])
+        else:
+            wait(rr.at[:, pl.ds(GJ * g, GJ)], ret_recv.at[g])
+        cs = slice(GR * g, GR * g + GR)
+        parts = []
+        tail = None
+        for k in range(3):
+            both = jnp.concatenate([comb[0, :, cs], comb[1 + k, :, cs]], axis=0)
+            v = dot(both, rr.at[k].reshape(512, T)[pl.ds(GR * g, GR), :])
+            parts.append(v[:T])
+            tail = v[T:] if k == 0 else tail + v[T:]
+        parts.append(tail)
+        moe = parts if g == 0 else [m + q for m, q in zip(moe, parts)]
+    for k in range(4):
         lg[0, :, 128 * k : 128 * k + 128] = (
-            cot[:, 128 * k : 128 * k + 128].astype(F32) + v[:T]
+            cot[:, 128 * k : 128 * k + 128].astype(F32) + moe[k]
         ).astype(BF)
-        tail = v[T:] if k == 0 else tail + v[T:]
-    lg[0, :, 384:512] = (cot[:, 384:512].astype(F32) + tail).astype(BF)
     remote(lg.at[0], lg.at[1], lg_send, lg_recv.at[0], right)
     remote(lg.at[0], lg.at[3], lg_send, lg_recv.at[1], left)
     loaded(10)
@@ -509,8 +569,7 @@
             lt.at[:, xx * NC + cc], rtm.at[:, :, pl.ds(T * p, T)], rt_send, rt_recv, (zz, xx, cc, y)
         )
     local(lt.at[:, plane], rtm.at[:, :, pl.ds(0, T)], self_sem.at[7])
-    ow_o[...] = (odf * ms[...].astype(F32) * (sig * (1.0 + ogf * (1.0 - sig)))).astype(BF)
-    local(ow_o, og_o, o_sem.at[7])
+    og_o[...] = (odf * ms[...].astype(F32) * (sig * (1.0 + ogf * (1.0 - sig)))).astype(BF)
 
     wsum = None
     for h in range(HEADS):
@@ -529,8 +588,7 @@
     got_states(wsw, 1)
     for h in range(HEADS):
         rgrad = rgrad + dot(dfi[h], wsw[pl.ds(8 * h, 8)].reshape(T, T), 1, 1)
-    ow_r[...] = rgrad.astype(BF)
-    local(ow_r, rg_o, o_sem.at[6])
+    rg_o[...] = rgrad.astype(BF)
 
     got_states(strd, 2)
     scan(strd, outr)
@@ -555,17 +613,14 @@
             p = dot(sw[...], state) * fts[h]
             u.append(p + pltpu.roll(p, 64, 1))
             wgrad = wgrad + dot(vfi[h], state, 1, 1)
-        ow_v[:, cols] = (vint[:, cols] + jnp.where(half, u[0], u[1])).astype(BF)
-    ow_w[...] = wgrad.astype(BF)
-    local(ow_v, vg_o, o_sem.at[4])
-    local(ow_w, wg_o, o_sem.at[5])
+        vg_o[:, cols] = (vint[:, cols] + jnp.where(half, u[0], u[1])).astype(BF)
+    wg_o[...] = wgrad.astype(BF)
 
     wait(zr.at[pl.ds(1, NZ - 1)], z_recv)
     total = pgown[z]
     for dz in range(1, NZ):
         total = total + zr[dz].astype(F32)
-    ow_p[...] = total
-    local(ow_p, pg_o, o_sem.at[3])
+    pg_o[...] = total
 
     wait(sx.at[:, pl.ds(1, NSP - 1)], d_send)
     wait(gy.at[pl.ds(1, 3)], y_send)
@@ -578,12 +633,6 @@
     wait(ga.at[pl.ds(1, PLANE - 1)], ga_send)
     wait(rtm.at[:, :, pl.ds(T, T * (PLANE - 1))], rt_send)
     wait(zr.at[pl.ds(1, NZ - 1)], z_send)
-    stores = (
-        (ow_gu.at[:, pl.ds(0, 256)], gg_o.at[0]), (ow_gu.at[:, pl.ds(256, 256)], ug_o.at[0]),
-        (ow_d, dg_o.at[0]), (ow_p, pg_o), (ow_v, vg_o), (ow_w, wg_o), (ow_r, rg_o), (ow_o, og_o),
-    )
-    for n, (a, b) in enumerate(stores):
-        pltpu.make_async_copy(a, b, o_sem.at[n]).wait()
 
 
 def bf(*shape):
@@ -619,9 +668,9 @@
     bf(512, 256),
     bf(3, 3, 64, 8, T),
     fl(3, 512, T),
-    bf(3, 32, 8, T),
-    bf(3, 32, 8, T),
-    bf(2, 3, 32, 8, T),
+    bf(GROUPS, 3, GJ // 2, 8, T),
+    bf(GROUPS, 3, GJ // 2, 8, T),
+    bf(2, GROUPS, 3, GJ // 2, 8, T),
     bf(3, 64, 8, T),
     bf(3, 64, 8, T),
     bf(3, 64, 8, T),
@@ -656,15 +705,7 @@
     bf(8, 32, W),
     bf(8, 32, W),
     fl(8, 32, W),
-    bf(2048, 512),
-    bf(256, 2048),
-    fl(32, W),
-    bf(T, W),
-    bf(T, T),
-    bf(T, T),
-    bf(T, W),
     sem(11),
-    sem(8),
     sem(9),
     pltpu.SemaphoreType.DMA,
     sem(8),
@@ -673,9 +714,9 @@
     sem(8),
     sem(8),
     pltpu.SemaphoreType.DMA,
-    sem(6),
-    pltpu.SemaphoreType.DMA,
-    pltpu.SemaphoreType.DMA,
+    sem(6 * GROUPS),
+    pltpu.SemaphoreType.DMA,
+    sem(GROUPS),
     pltpu.SemaphoreType.DMA,
     sem(4),
     sem(5),
@@ -695,25 +736,44 @@
 ):
     hbm = pl.BlockSpec(memory_space=pl.ANY)
     vmem = pl.BlockSpec(memory_space=pltpu.VMEM)
-    shape = jax.ShapeDtypeStruct
-    return pl.pallas_call(
+    shapes = (
+        ((1, 2048, 256), BF), ((1, 2048, 256), BF), ((1, 256, 2048), BF), ((32, W), F32),
+        ((T, W), BF), ((T, T), BF), ((T, T), BF), ((T, W), BF),
+    )
+    results = pl.pallas_call(
         body,
         name="layer_backward",
-        out_shape=(
-            shape((1, 2048, 256), BF), shape((1, 2048, 256), BF), shape((1, 256, 2048), BF),
-            shape((32, W), F32), shape((T, W), BF), shape((T, T), BF), shape((T, T), BF),
-            shape((T, W), BF),
-        ),
+        out_shape=tuple(pltpu.VMEM(s, t) for s, t in shapes),
         in_specs=[hbm, hbm, vmem, vmem] + [hbm] * 9 + [vmem],
-        out_specs=tuple([hbm] * 8),
+        out_specs=tuple([vmem] * 8),
         scratch_shapes=SCRATCH,
         compiler_params=pltpu.CompilerParams(
-            collective_id=0, has_side_effects=True, vmem_limit_bytes=60 * 1024 * 1024
+            collective_id=0, has_side_effects=True, vmem_limit_bytes=52 * 1024 * 1024
         ),
     )(
         layer_input, cotangent, routes.T, route_weight.T, gate_weight, up_weight, down_weight,
         heads_value, output_gate, mixer_saved, proj_weight, state_write, state_read, decay_rate.T,
     )
+
+    def store(*refs):
+        sems = refs[-1]
+        copies = [
+            pltpu.make_async_copy(refs[n], refs[8 + n], sems.at[n]) for n in range(8)
+        ]
+        for copy in copies:
+            copy.start()
+        for copy in copies:
+            copy.wait()
+
+    return pl.pallas_call(
+        store,
+        name="store",
+        out_shape=tuple(jax.ShapeDtypeStruct(s, t) for s, t in shapes),
+        in_specs=[vmem] * 8,
+        out_specs=tuple([hbm] * 8),
+        scratch_shapes=[sem(8)],
+        compiler_params=pltpu.CompilerParams(vmem_limit_bytes=8 * 1024 * 1024),
+    )(*results)
 
 
 def solution(mesh):

time: 125 us -> 112 us (0.90)
  local copies, waits for them, and re-layouts: 7.55 us -> 0 us
  Pallas kernels: 116 us -> 111 us
    unnamed x22 -> x0, local copies, waits for them, and re-layouts: 7.55 us -> none
    pallas_call x1 -> x2, Pallas kernels: 116 us -> 111 us  [the longest x1 109 us: on_device(): pl.pallas_call(body, name='layer_backward', out_shape=tuple((pltpu.VMEM(s...]
where the time goes in v2:
time: 112 us
  Pallas kernels  111 us (99%)
    pallas_call x1, Pallas kernels, on_device(): pl.pallas_call(body, name='layer_backward', out_shape=tuple((pltpu.VMEM(s...  109 us

profile of v2, /device:TPU:24, one launch (start us, length us, event | category | flops | bytes accessed | tf_op | source)
XLA Modules:
  0.0 111.7 jit_solution(12369114993253353433)
XLA Ops:
  0.6 109.2 %layer_backward.1 = (bf16[1,2048,256]{2,1,0:T(8,128)(2,1)S(1)}, bf16[1,2048,256]{2,1,0:T(8,128)(2,1)S(1)}, bf16[1,256,2048]{2,1,0:T(8,128)(2,1)S(1)}, f32[32,512...) custom-call(bf16[128,512]{1,0:T(8,128)(2,1)} %li_h.1, ...), custom_call_target="tpu_custom_call" | custom-call | tf_op jit(solution)/shard_map/layer_backward/pallas_call | solution.py:743
  109.9 1.9 %store.1 = (bf16[1,2048,256]{2,1,0:T(8,128)(2,1)}, bf16[1,2048,256]{2,1,0:T(8,128)(2,1)}, bf16[1,256,2048]{2,1,0:T(8,128)(2,1)}, f32[32,512]{1,0:T(8,128)}, bf16...) custom-call(bf16[1,2048,256]{2,1,0:T(8,128)(2,1)S(1)} %get-tuple-element.1, ...), custom_call_target="tpu_custom_call" | custom-call | tf_op jit(solution)/shard_map/store/pallas_call | solution.py:768

commit v3 on v2

--- a/solution.py
+++ b/solution.py
@@ -16,8 +16,10 @@
 CAP = 6
 BF = jnp.bfloat16
 F32 = jnp.float32
-ORDER = (0, 1, 7, 2, 6, 3, 5, 4)
-GROUPS = 2
+ORDER = (0, 2, 6, 5, 3, 4, 7, 1)
+PACKED = sum(d << (3 * n) for n, d in enumerate(ORDER))
+PLACES = sum(n << (3 * d) for n, d in enumerate(ORDER))
+GROUPS = 4
 GC = NZ // GROUPS
 GJ = GC * PLANE
 GR = GJ * 8
@@ -36,18 +38,17 @@
 
 
 def body(
-    li_h, cot_h, rt_v, rw_v, gw_h, uw_h, dw_h, hv_h, og_h, ms_h, pw_h, sw_h, sr_h, dr_v,
+    li_h, cot_h, rt_h, rw_h, gw_h, uw_h, dw_h, hv_h, og_h, ms_h, pw_h, sw_h, sr_h, dr_h,
     gg_o, ug_o, dg_o, pg_o, vg_o, wg_o, rg_o, og_o,
     *scratch,
 ):
     (
-        li, cot, gu, dw, hv, og, ms, pw, sw, sr, sx, gy, xm, cm, acc_gu, acc_h, gud, hid, ps,
-        own, hl, hr, mrg, nl, nr, ret, rr, comb, lg, od, dl, sstw, sstr, stw, strd, low, high,
-        outw, outr, wsw, wsr, fsend, frecv, vfs, vfi, dfs, dfi, fts, lst, lker, vint, lt, rtm,
-        ga, pgs, zr, pgown, ld_sem, self_sem,
+        rt_v, rw_v, dr_v, li, cot, gu, dw, hv, og, ms, pw, sw, sr, sx, gy, xm, cm, acc_gu, acc_h, gud, hid, ps,
+        own, hl, hr, mrg, nl, nr, ret, rr, comb, lg, od, dl, sstw, sstr, low, inb, zs, zb, outb, fplane, fade_send, fade_recv,
+        wsw, wsr, fsend, frecv, vfs, vfi, dfs, dfi, fts, lst, lker, vint, lt, rtm,
+        ga, pgs, zr, pgown, ld_sem, self_sem, in_sem, out_sem,
         d_send, d_recv, y_send, yl_recv, yr_recv, yo_recv, rs_send, rs_recv, ret_send, ret_recv,
         lg_send, lg_recv, st_send, st_recv, ga_send, ga_recv, rt_send, rt_recv, z_send, z_recv,
-
     ) = scratch
     z = lax.axis_index("sp_0")
     x = lax.axis_index("sp_1")
@@ -87,12 +88,16 @@
         pltpu.make_async_copy(ref, ref, sem).wait()
 
     def dz_of(n):
-        odd = lax.rem(n, 2)
-        return lax.rem(odd * ((n + 1) // 2) + (1 - odd) * (NZ - n // 2), NZ)
+        return lax.shift_right_logical(jnp.int32(PACKED), 3 * n) & 7
 
     def n_of(dz):
-        far = dz // 5
-        return (1 - far) * (2 * dz - 1) + far * (16 - 2 * dz) + (NZ - dz) // NZ
+        return lax.shift_right_logical(jnp.int32(PLACES), 3 * dz) & 7
+
+    def dz_vec(n):
+        out = jnp.zeros_like(n)
+        for k, d in enumerate(ORDER):
+            out = jnp.where(n == k, d, out)
+        return out
 
     def to_all(send, first=0, last=NZ):
         if first == 0:
@@ -110,10 +115,10 @@
     loads = (
         (li_h, li), (cot_h, cot), (hv_h, hv), (sw_h, sw), (sr_h, sr), (og_h, og), (ms_h, ms),
         (gw_h.at[0], gu.at[:, pl.ds(0, 256)]), (uw_h.at[0], gu.at[:, pl.ds(256, 256)]),
-        (dw_h.at[0], dw), (pw_h, pw),
+        (dw_h.at[0], dw), (pw_h, pw), (rt_h, rt_v), (rw_h, rw_v), (dr_h, dr_v),
     )
-    for n, (a, b) in enumerate(loads):
-        local(a, b, ld_sem.at[n])
+    for n in (11, 12, 13, 0, 1, 2, 3, 4, 5, 6, 7, 8, 9, 10):
+        local(*loads[n], ld_sem.at[n])
 
     def loaded(n):
         wait(loads[n][1], ld_sem.at[n])
@@ -128,11 +133,14 @@
     greet(left)
     greet(opposite)
 
+    loaded(11)
+    loaded(12)
+    loaded(13)
     ci = iota((512, T), 0)
     r8 = lax.rem(ci, 8)
     blk = ci // 8
     e = (
-        lax.rem(z + dz_of(blk // PLANE), NZ) * PLANE
+        lax.rem(z + dz_vec(blk // PLANE), NZ) * PLANE
         + lax.rem(x + lax.rem(blk // NC, NX), NX) * NC
         + lax.rem(c + lax.rem(blk, NC), NC)
     )
@@ -206,25 +214,117 @@
     def states(vectors_t, first, dst):
         for h in range(0, HEADS, 2):
             s = dot(vectors_t, jnp.concatenate([first[h], first[h + 1]], axis=1))
-            dst[pl.ds(8 * h, 8)] = s[:, :T].astype(BF).reshape(8, 16, T)
-            dst[pl.ds(8 * h + 8, 8)] = s[:, T:].astype(BF).reshape(8, 16, T)
+            dst[h] = s[:, :T].astype(BF)
+            dst[h + 1] = s[:, T:].astype(BF)
 
     swt = sw[...].astype(F32).T.astype(BF)
     states(swt, vfs, sstw)
 
-    def send_state(src, dst, n):
-        def go(n_, dz, p):
-            zz, xx, cc = ahead(dz, p)
-            j = n_ * PLANE + p
-            remote(src.at[zz * PLANE + xx * NC + cc], dst.at[j], st_send.at[n], st_recv.at[n], (zz, xx, cc, y))
-
-        local(src.at[me], dst.at[0], self_sem.at[1 + n])
-        to_all(go)
+    def place(i):
+        return lax.rem(x + NX - i // NC, NX) * NC + lax.rem(c + i % NC, NC)
+
+    def rowhalf(u):
+        return pl.ds(64 * u, 64)
+
+    quarter = iota((32, T), 1) < 64
+
+    def packed_half(v, at_left):
+        other = pltpu.roll(v[:32] if not at_left else v[32:], 64, 1)
+        return jnp.where(quarter, v[:32] if at_left else other, other if at_left else v[32:])
+
+    def send_plane(src, e):
+        for u in range(2):
+            k = 6 * e + 3 * u
+            for p in range(1, PLANE):
+                zz, xx, cc = ahead(0, p)
+                remote(
+                    src.at[xx * NC + cc, rowhalf(u)], inb.at[e, u, p], st_send.at[k], st_recv.at[k],
+                    (zz, xx, cc, y),
+                )
+            local(src.at[plane, rowhalf(u)], inb.at[e, u, 0], in_sem.at[2 * e + u])
+
+    def plane_totals(e, u):
+        k = 6 * e + 3 * u
+        wait(inb.at[e, u, pl.ds(1, PLANE - 1)], st_recv.at[k])
+        wait(inb.at[e, u, 0], in_sem.at[2 * e + u])
+        up = None
+        down = None
+        for i in range(PLANE):
+            p = place(i)
+            q = place(PLANE - 1 - i)
+            v = inb[e, u, p].astype(F32)
+            w = inb[e, u, q].astype(F32)
+            up = v if i == 0 else up * frecv[p] + v
+            down = w if i == 0 else down * frecv[q] + w
+        zs[e, u, 0] = packed_half(up, True).astype(BF)
+        zs[e, u, 1] = packed_half(down, False).astype(BF)
+        for dz in (4, 5, 3, 6, 2, 1, 7):
+            zz = lax.rem(z + dz, NZ)
+            remote(
+                zs.at[e, u, (z + dz) // NZ], zb.at[e, u, dz], st_send.at[k + 1], st_recv.at[k + 1],
+                (zz, x, c, y),
+            )
+
+    def spread(e, u, dst):
+        k = 6 * e + 3 * u
+        wait(zb.at[e, u, pl.ds(1, NZ - 1)], st_recv.at[k + 1])
+        up = jnp.zeros((32, T), F32)
+        down = jnp.zeros((32, T), F32)
+        for i in range(NZ):
+            dz = lax.rem(z + NZ - i, NZ)
+            f = fplane[n_of(dz)]
+            v = zb[e, u, dz].astype(F32)
+            up = jnp.where((z - i + NZ - 1) // NZ == 1, up * f + v, up)
+            r = NZ - 1 - i
+            dz = lax.rem(z + NZ - r, NZ)
+            f = fplane[n_of(dz)]
+            v = zb[e, u, dz].astype(F32)
+            down = jnp.where((r - z + NZ - 1) // NZ == 1, down * f + v, down)
+        start = jnp.concatenate(
+            [
+                jnp.where(quarter, up, pltpu.roll(down, 64, 1)),
+                jnp.where(quarter, pltpu.roll(up, 64, 1), down),
+            ],
+            axis=0,
+        )
+        cur = start
+        for i in range(PLANE):
+            p = place(i)
+            low[p] = cur
+            if i < PLANE - 1:
+                cur = cur * frecv[p] + inb[e, u, p].astype(F32)
+        cur = start
+        for i in reversed(range(PLANE)):
+            p = place(i)
+            outb[e, u, p] = jnp.where(half[:64], low[p], cur).astype(BF)
+            if i > 0:
+                cur = cur * frecv[p] + inb[e, u, p].astype(F32)
+        for p in range(1, PLANE):
+            zz, xx, cc = behind(0, p)
+            remote(
+                outb.at[e, u, p], dst.at[plane, rowhalf(u)], st_send.at[k + 2], st_recv.at[k + 2],
+                (zz, xx, cc, y),
+            )
+        local(outb.at[e, u, 0], dst.at[plane, rowhalf(u)], out_sem.at[2 * e + u])
+
+    def got_states(ref, e):
+        for u in range(2):
+            wait(inb.at[e, u, pl.ds(1, PLANE - 1)], st_recv.at[6 * e + 3 * u + 2])
+            wait(ref.at[0, rowhalf(u)], out_sem.at[2 * e + u])
+
+    def fades_here():
+        wait(frecv.at[pl.ds(1, NSP - 1)], fade_recv)
+        wait(frecv.at[0], self_sem.at[5])
+        for n in range(NZ):
+            f = frecv[PLANE * n]
+            for p in range(1, PLANE):
+                f = f * frecv[PLANE * n + p]
+            fplane[n] = f
 
     def send_fade(n, dz, p):
         zz, xx, cc = ahead(dz, p)
         j = n * PLANE + p
-        remote(fsend.at[zz], frecv.at[j], st_send.at[4], st_recv.at[4], (zz, xx, cc, y))
+        remote(fsend.at[xx * NC + cc], frecv.at[j], fade_send, fade_recv, (zz, xx, cc, y))
 
     loaded(5)
     loaded(6)
@@ -240,9 +340,12 @@
     local(sx.at[:, 0], gy.at[0, :, 0], self_sem.at[0])
     to_all(send_x)
 
-    local(fsend.at[z], frecv.at[0], self_sem.at[5])
+    local(fsend.at[plane], frecv.at[0], self_sem.at[5])
+    for e in range(2):
+        for u in range(2):
+            zb[e, u, 0] = jnp.zeros((32, T), BF)
     to_all(send_fade)
-    send_state(sstw, stw, 0)
+    send_plane(sstw, 0)
 
     for p in range(1, PLANE):
         remote(ga.at[0], ga.at[p], ga_send, ga_recv, ahead(0, p) + (y,))
@@ -398,104 +501,86 @@
             local(ret.at[:, 0], rr.at[:, 0], self_sem.at[6])
         to_all(send_back, GC * g, GC * g + GC)
 
-    for n in range(4):
-        arrived(n)
-        if n >= 2:
-            forward(n - 2)
-    loaded(7)
-    loaded(8)
-    loaded(9)
-    arrived(4)
-    forward(2)
-    expert_in(0, 0)
-    arrived(5)
-    forward(3)
-    expert_in(0, 1)
-    arrived(6)
-    forward(4)
-    expert_in(0, 3)
-    arrived(7)
-    forward(5)
-    expert_in(0, 2)
-    forward(6)
-    activations(0)
-    forward(7)
-    far_partials(0)
-    right_partials(0)
-    left_partials(0)
-    expert_in(1, 0)
-    merge(0)
-    expert_in(1, 1)
-    packed(0, 0, put_own)
-    expert_in(1, 3)
-    expert_in(1, 2)
-    activations(1)
-    far_partials(1)
-    right_partials(1)
-    left_partials(1)
-    give_back(0)
-    merge(1)
-    packed(1, 0, put_own)
-
-    def scan(b, out):
-        def at(i):
-            return (
-                n_of(lax.rem(z + NZ - i // PLANE, NZ)) * PLANE
-                + lax.rem(x + NX - lax.rem(i // NC, NX), NX) * NC
-                + lax.rem(c + lax.rem(i, NC), NC)
-            )
-
-        def step(n, carry):
-            s, t = carry
-            jf = at(n)
-            jb = at(NSP - 1 - n)
-            low[jf] = s
-            s = s * frecv[jf] + b[jf].astype(F32)
-            high[jb] = t
-            t = t * frecv[jb] + b[jb].astype(F32)
-            return s, t
-
-        zero = jnp.zeros((16, T), F32)
-        lax.fori_loop(0, NSP, step, (zero, zero))
-
-        def join(n, _):
-            pos = pl.ds(n * 8, 8)
-            out[pos] = jnp.where(iota((8, 16, T), 2) < 64, low[pos], high[pos]).astype(BF)
-            return 0
-
-        lax.fori_loop(0, 8, join, 0)
-
-    def states_back(out, dst, n):
-        def go(n_, dz, p):
-            zz, xx, cc = behind(dz, p)
-            j = n_ * PLANE + p
-            remote(out.at[j], dst.at[me], st_send.at[n], st_recv.at[n], (zz, xx, cc, y))
-
-        local(out.at[0], dst.at[me], self_sem.at[1 + n])
-        to_all(go)
-
-    def got_states(ref, n):
-        wait(ref.at[pl.ds(1, NSP - 1)], st_recv.at[n])
-        wait(ref.at[0], self_sem.at[1 + n])
-
-    wait(frecv.at[pl.ds(1, NSP - 1)], st_recv.at[4])
-    wait(frecv.at[0], self_sem.at[5])
-    got_states(stw, 0)
-    scan(stw, outw)
-
-    give_back(1)
-    states_back(outw, wsw, 1)
-
-    def weight_grad(n, _):
-        cols = pl.ds(pl.multiple_of(n * 256, 256), 256)
-        src = pl.multiple_of(lax.rem(y + NY - n // 2, NY) * 512 + lax.rem(n, 2) * 256, 256)
+    def partials(g):
+        activations(g)
+        far_partials(g)
+        right_partials(g)
+        left_partials(g)
+
+    def own_partials(g):
+        packed(g, 0, put_own)
+
+    def weight_grad(n):
+        cols = pl.ds(256 * n, 256)
+        src = pl.multiple_of(lax.rem(y + NY - n // 2, NY) * 512 + (n % 2) * 256, 256)
         both = dot(xm[:, cols], gud[...], 0, 0).astype(BF)
         gg_o[0, pl.ds(src, 256), :] = both[:, :256]
         ug_o[0, pl.ds(src, 256), :] = both[:, 256:]
         dg_o[0, :, pl.ds(src, 256)] = dot(hid[...], cm[:, cols], 0, 0).astype(BF)
-        return 0
-
-    lax.fori_loop(0, 8, weight_grad, 0)
+
+    arrived(0)
+    arrived(1)
+    forward(0)
+    arrived(2)
+    forward(1)
+    loaded(7)
+    loaded(8)
+    loaded(9)
+    expert_in(0, 0)
+    expert_in(0, 1)
+    expert_in(0, 3)
+    arrived(3)
+    forward(2)
+    expert_in(0, 2)
+    partials(0)
+    arrived(4)
+    forward(3)
+    expert_in(1, 0)
+    expert_in(1, 1)
+    expert_in(1, 3)
+    arrived(5)
+    fades_here()
+    plane_totals(0, 0)
+    plane_totals(0, 1)
+    forward(4)
+    merge(0)
+    expert_in(1, 2)
+    partials(1)
+    own_partials(0)
+    arrived(6)
+    forward(5)
+    arrived(7)
+    spread(0, 0, wsw)
+    spread(0, 1, wsw)
+    forward(6)
+    expert_in(2, 0)
+    expert_in(2, 1)
+    expert_in(2, 3)
+    forward(7)
+    merge(1)
+    expert_in(2, 2)
+    partials(2)
+    own_partials(1)
+    expert_in(3, 0)
+    expert_in(3, 1)
+    expert_in(3, 3)
+    give_back(0)
+    expert_in(3, 2)
+    partials(3)
+    own_partials(2)
+    merge(2)
+    own_partials(3)
+    give_back(1)
+    weight_grad(0)
+    weight_grad(1)
+    merge(3)
+    weight_grad(2)
+    give_back(2)
+    weight_grad(3)
+    give_back(3)
+
+    for n in range(4, 6):
+        weight_grad(n)
     common_t = dot(sw[...], sr[...], 1, 1)
     for h in range(HEADS):
         lst[h] = (lker[h] * common_t).astype(BF)
@@ -521,8 +606,12 @@
         lg[0, :, 128 * k : 128 * k + 128] = (
             cot[:, 128 * k : 128 * k + 128].astype(F32) + moe[k]
         ).astype(BF)
-    remote(lg.at[0], lg.at[1], lg_send, lg_recv.at[0], right)
-    remote(lg.at[0], lg.at[3], lg_send, lg_recv.at[1], left)
+    first = pl.ds(0, 64)
+    second = pl.ds(64, 64)
+    remote(lg.at[0, first], lg.at[1, first], lg_send, lg_recv.at[0], right)
+    remote(lg.at[0, second], lg.at[3, second], lg_send, lg_recv.at[1], left)
+    remote(lg.at[0, second], lg.at[1, second], lg_send, lg_recv.at[2], right)
+    remote(lg.at[0, first], lg.at[3, first], lg_send, lg_recv.at[3], left)
     loaded(10)
 
     def out_part(d):
@@ -533,23 +622,34 @@
             od[...] += v
 
     def transposed(d):
+        yy = lax.rem(y + NY - d, NY)
         for q in range(4):
             blkt = lg[d, :, 128 * q : 128 * q + 128].astype(F32).T.astype(BF)
-            zz = lax.rem(y + NY - d, NY) * 2 + q // 2
-            lt[zz, pl.ds(4 * (q % 2), 4)] = blkt.reshape(4, 32, T)
+            lt[yy * 2 + q // 2, pl.ds(4 * (q % 2), 4)] = blkt.reshape(4, 32, T)
+        pair = pl.ds(yy * 2, 2)
+        for p in range(1, PLANE):
+            zz, xx, cc = ahead(0, p)
+            remote(
+                lt.at[pair, xx * NC + cc], rtm.at[pair, :, pl.ds(T * p, T)], rt_send, rt_recv,
+                (zz, xx, cc, y),
+            )
 
     out_part(0)
-    wait(lg.at[1], lg_recv.at[0])
-    remote(lg.at[1, pl.ds(0, 64)], lg.at[2, pl.ds(0, 64)], lg_send, lg_recv.at[2], right)
-    wait(lg.at[3], lg_recv.at[1])
-    remote(lg.at[3, pl.ds(64, 64)], lg.at[2, pl.ds(64, 64)], lg_send, lg_recv.at[3], left)
+    weight_grad(6)
+    weight_grad(7)
+    wait(lg.at[1, first], lg_recv.at[0])
+    remote(lg.at[1, first], lg.at[2, first], lg_send, lg_recv.at[4], right)
+    wait(lg.at[3, second], lg_recv.at[1])
+    remote(lg.at[3, second], lg.at[2, second], lg_send, lg_recv.at[5], left)
+    transposed(0)
+    wait(lg.at[1, second], lg_recv.at[2])
+    wait(lg.at[3, first], lg_recv.at[3])
     out_part(1)
     out_part(3)
-    transposed(0)
     transposed(1)
     transposed(3)
-    wait(lg.at[2, pl.ds(0, 64)], lg_recv.at[2])
-    wait(lg.at[2, pl.ds(64, 64)], lg_recv.at[3])
+    wait(lg.at[2, first], lg_recv.at[4])
+    wait(lg.at[2, second], lg_recv.at[5])
     out_part(2)
     odf = od[...].astype(BF).astype(F32)
     ogf = og[...].astype(F32)
@@ -561,13 +661,8 @@
     sides(lambda k: od[:, 128 * k : 128 * k + 128], dfs, dfi)
     srt = sr[...].astype(F32).T.astype(BF)
     states(srt, dfs, sstr)
-    send_state(sstr, strd, 2)
+    send_plane(sstr, 1)
     transposed(2)
-    for p in range(1, PLANE):
-        zz, xx, cc = ahead(0, p)
-        remote(
-            lt.at[:, xx * NC + cc], rtm.at[:, :, pl.ds(T * p, T)], rt_send, rt_recv, (zz, xx, cc, y)
-        )
     local(lt.at[:, plane], rtm.at[:, :, pl.ds(0, T)], self_sem.at[7])
     og_o[...] = (odf * ms[...].astype(F32) * (sig * (1.0 + ogf * (1.0 - sig)))).astype(BF)
 
@@ -585,14 +680,12 @@
         a = dot(lst[2 * k], dl[:, cols])
         b = dot(lst[2 * k + 1], dl[:, cols])
         vint[:, cols] = jnp.where(half, a, b)
-    got_states(wsw, 1)
+    plane_totals(1, 0)
+    plane_totals(1, 1)
+    got_states(wsw, 0)
     for h in range(HEADS):
-        rgrad = rgrad + dot(dfi[h], wsw[pl.ds(8 * h, 8)].reshape(T, T), 1, 1)
+        rgrad = rgrad + dot(dfi[h], wsw[h], 1, 1)
     rg_o[...] = rgrad.astype(BF)
-
-    got_states(strd, 2)
-    scan(strd, outr)
-    states_back(outr, wsr, 3)
 
     wait(ga.at[pl.ds(1, PLANE - 1)], ga_recv)
     wait(rtm.at[:, :, pl.ds(T, T * (PLANE - 1))], rt_recv)
@@ -604,12 +697,14 @@
         zz = lax.rem(z + dz, NZ)
         remote(pgs.at[zz], zr.at[dz], z_send, z_recv, (zz, x, c, y))
 
-    got_states(wsr, 3)
+    spread(1, 0, wsr)
+    spread(1, 1, wsr)
+    got_states(wsr, 1)
     for k in range(HEADS // 2):
         cols = slice(128 * k, 128 * k + 128)
         u = []
         for h in (2 * k, 2 * k + 1):
-            state = wsr[pl.ds(8 * h, 8)].reshape(T, T)
+            state = wsr[h]
             p = dot(sw[...], state) * fts[h]
             u.append(p + pltpu.roll(p, 64, 1))
             wgrad = wgrad + dot(vfi[h], state, 1, 1)
@@ -627,9 +722,11 @@
     wait(ps, rs_send)
     wait(ret.at[:, pl.ds(1, NSP - 1)], ret_send)
     wait(lg.at[pl.ds(0, 3)], lg_send)
-    for n in range(4):
-        wait(stw.at[pl.ds(1, NSP - 1)], st_send.at[n])
-    wait(frecv.at[pl.ds(1, NSP - 1)], st_send.at[4])
+    for k in range(4):
+        wait(inb.at[k // 2, k % 2, pl.ds(1, PLANE - 1)], st_send.at[3 * k])
+        wait(zb.at[k // 2, k % 2, pl.ds(1, NZ - 1)], st_send.at[3 * k + 1])
+        wait(inb.at[k // 2, k % 2, pl.ds(1, PLANE - 1)], st_send.at[3 * k + 2])
+    wait(frecv.at[pl.ds(1, NSP - 1)], fade_send)
     wait(ga.at[pl.ds(1, PLANE - 1)], ga_send)
     wait(rtm.at[:, :, pl.ds(T, T * (PLANE - 1))], rt_send)
     wait(zr.at[pl.ds(1, NZ - 1)], z_send)
@@ -648,6 +745,9 @@
 
 
 SCRATCH = (
+    pltpu.VMEM((2, T), jnp.int32),
+    fl(2, T),
+    fl(8, T),
     bf(T, W),
     bf(T, W),
     bf(2048, 512),
@@ -679,16 +779,18 @@
     bf(4, T, W),
     fl(T, W),
     bf(T, W),
-    bf(64, 16, T),
-    bf(64, 16, T),
-    bf(64, 16, T),
-    bf(64, 16, T),
-    fl(64, 16, T),
-    fl(64, 16, T),
-    bf(64, 16, T),
-    bf(64, 16, T),
-    bf(64, 16, T),
-    bf(64, 16, T),
+    bf(8, T, T),
+    bf(8, T, T),
+    fl(8, 64, T),
+    bf(2, 2, 8, 64, T),
+    bf(2, 2, 2, 32, T),
+    bf(2, 2, 8, 32, T),
+    bf(2, 2, 8, 64, T),
+    fl(8, 1, T),
+    pltpu.SemaphoreType.DMA,
+    pltpu.SemaphoreType.DMA,
+    bf(8, T, T),
+    bf(8, T, T),
     fl(8, 1, T),
     fl(64, 1, T),
     bf(8, T, T),
@@ -705,8 +807,10 @@
     bf(8, 32, W),
     bf(8, 32, W),
     fl(8, 32, W),
-    sem(11),
+    sem(14),
     sem(9),
+    sem(4),
+    sem(4),
     pltpu.SemaphoreType.DMA,
     sem(8),
     pltpu.SemaphoreType.DMA,
@@ -718,9 +822,9 @@
     pltpu.SemaphoreType.DMA,
     sem(GROUPS),
     pltpu.SemaphoreType.DMA,
-    sem(4),
-    sem(5),
-    sem(5),
+    sem(6),
+    sem(12),
+    sem(12),
     pltpu.SemaphoreType.DMA,
     pltpu.SemaphoreType.DMA,
     pltpu.SemaphoreType.DMA,
@@ -744,7 +848,7 @@
         body,
         name="layer_backward",
         out_shape=tuple(pltpu.VMEM(s, t) for s, t in shapes),
-        in_specs=[hbm, hbm, vmem, vmem] + [hbm] * 9 + [vmem],
+        in_specs=[hbm] * 14,
         out_specs=tuple([vmem] * 8),
         scratch_shapes=SCRATCH,
         compiler_params=pltpu.CompilerParams(

time: 112 us -> 99 us (0.88)
  Pallas kernels: 111 us -> 97.2 us
    pallas_call x1, Pallas kernels: 109 us -> 95.3 us  [on_device(): pl.pallas_call(body, name='layer_backward', out_shape=tuple((pltpu.VMEM(s...]
where the time goes in v3:
time: 99 us; the launch traced here: 98 us
  Pallas kernels  97.2 us (98%)
    pallas_call x1, Pallas kernels, on_device(): pl.pallas_call(body, name='layer_backward', out_shape=tuple((pltpu.VMEM(s...  95.3 us

profile of v3, /device:TPU:24, one launch (start us, length us, event | category | flops | bytes accessed | tf_op | source)
XLA Modules:
  0.0 98.0 jit_solution(15770569793484198349)
XLA Ops:
  0.6 95.3 %layer_backward.1 = (bf16[1,2048,256]{2,1,0:T(8,128)(2,1)S(1)}, bf16[1,2048,256]{2,1,0:T(8,128)(2,1)S(1)}, bf16[1,256,2048]{2,1,0:T(8,128)(2,1)S(1)}, f32[32,512...) custom-call(bf16[128,512]{1,0:T(8,128)(2,1)} %li_h.1, ...), custom_call_target="tpu_custom_call" | custom-call | tf_op jit(solution)/shard_map/layer_backward/pallas_call | solution.py:847
  96.0 1.9 %store.1 = (bf16[1,2048,256]{2,1,0:T(8,128)(2,1)}, bf16[1,2048,256]{2,1,0:T(8,128)(2,1)}, bf16[1,256,2048]{2,1,0:T(8,128)(2,1)}, f32[32,512]{1,0:T(8,128)}, bf16...) custom-call(bf16[1,2048,256]{2,1,0:T(8,128)(2,1)S(1)} %get-tuple-element.1, ...), custom_call_target="tpu_custom_call" | custom-call | tf_op jit(solution)/shard_map/store/pallas_call | solution.py:872

commit v4 on v3

--- a/solution.py
+++ b/solution.py
@@ -16,7 +16,7 @@
 CAP = 6
 BF = jnp.bfloat16
 F32 = jnp.float32
-ORDER = (0, 2, 6, 5, 3, 4, 7, 1)
+ORDER = (0, 1, 6, 3, 5, 4, 2, 7)
 PACKED = sum(d << (3 * n) for n, d in enumerate(ORDER))
 PLACES = sum(n << (3 * d) for n, d in enumerate(ORDER))
 GROUPS = 4
@@ -46,7 +46,7 @@
         rt_v, rw_v, dr_v, li, cot, gu, dw, hv, og, ms, pw, sw, sr, sx, gy, xm, cm, acc_gu, acc_h, gud, hid, ps,
         own, hl, hr, mrg, nl, nr, ret, rr, comb, lg, od, dl, sstw, sstr, low, inb, zs, zb, outb, fplane, fade_send, fade_recv,
         wsw, wsr, fsend, frecv, vfs, vfi, dfs, dfi, fts, lst, lker, vint, lt, rtm,
-        ga, pgs, zr, pgown, ld_sem, self_sem, in_sem, out_sem,
+        ga, pgs, zr, pgown, ld_sem,
         d_send, d_recv, y_send, yl_recv, yr_recv, yo_recv, rs_send, rs_recv, ret_send, ret_recv,
         lg_send, lg_recv, st_send, st_recv, ga_send, ga_recv, rt_send, rt_recv, z_send, z_recv,
     ) = scratch
@@ -73,7 +73,6 @@
 
     right = (z, x, c, lax.rem(y + 1, NY))
     left = (z, x, c, lax.rem(y + NY - 1, NY))
-    opposite = (z, x, c, lax.rem(y + 2, NY))
 
     def remote(src, dst, ss, rs, dev):
         pltpu.make_async_remote_copy(
@@ -131,8 +130,10 @@
     to_all(lambda n, dz, p: greet(ahead(dz, p) + (y,)))
     greet(right)
     greet(left)
-    greet(opposite)
-
+
+    for e in range(2):
+        for u in range(2):
+            zb[e, u, 0] = jnp.zeros((32, T), BF)
     loaded(11)
     loaded(12)
     loaded(13)
@@ -238,15 +239,14 @@
             for p in range(1, PLANE):
                 zz, xx, cc = ahead(0, p)
                 remote(
-                    src.at[xx * NC + cc, rowhalf(u)], inb.at[e, u, p], st_send.at[k], st_recv.at[k],
+                    src.at[xx * NC + cc, rowhalf(u)], inb.at[e, u, p], st_send.at[0], st_recv.at[k],
                     (zz, xx, cc, y),
                 )
-            local(src.at[plane, rowhalf(u)], inb.at[e, u, 0], in_sem.at[2 * e + u])
+            inb[e, u, 0] = src[plane, rowhalf(u)]
 
     def plane_totals(e, u):
         k = 6 * e + 3 * u
         wait(inb.at[e, u, pl.ds(1, PLANE - 1)], st_recv.at[k])
-        wait(inb.at[e, u, 0], in_sem.at[2 * e + u])
         up = None
         down = None
         for i in range(PLANE):
@@ -261,7 +261,7 @@
         for dz in (4, 5, 3, 6, 2, 1, 7):
             zz = lax.rem(z + dz, NZ)
             remote(
-                zs.at[e, u, (z + dz) // NZ], zb.at[e, u, dz], st_send.at[k + 1], st_recv.at[k + 1],
+                zs.at[e, u, (z + dz) // NZ], zb.at[e, u, dz], st_send.at[1], st_recv.at[k + 1],
                 (zz, x, c, y),
             )
 
@@ -302,19 +302,17 @@
         for p in range(1, PLANE):
             zz, xx, cc = behind(0, p)
             remote(
-                outb.at[e, u, p], dst.at[plane, rowhalf(u)], st_send.at[k + 2], st_recv.at[k + 2],
+                outb.at[e, u, p], dst.at[plane, rowhalf(u)], st_send.at[2], st_recv.at[k + 2],
                 (zz, xx, cc, y),
             )
-        local(outb.at[e, u, 0], dst.at[plane, rowhalf(u)], out_sem.at[2 * e + u])
+        dst[plane, rowhalf(u)] = outb[e, u, 0]
 
     def got_states(ref, e):
         for u in range(2):
             wait(inb.at[e, u, pl.ds(1, PLANE - 1)], st_recv.at[6 * e + 3 * u + 2])
-            wait(ref.at[0, rowhalf(u)], out_sem.at[2 * e + u])
 
     def fades_here():
         wait(frecv.at[pl.ds(1, NSP - 1)], fade_recv)
-        wait(frecv.at[0], self_sem.at[5])
         for n in range(NZ):
             f = frecv[PLANE * n]
             for p in range(1, PLANE):
@@ -331,24 +329,14 @@
     ogf = og[...].astype(F32)
     sig = jax.nn.sigmoid(ogf)
     ga[0] = (ms[...].astype(F32) * (ogf * sig)).astype(BF)
-    pl.semaphore_wait(bar, NSP - 1 + 3)
+    pl.semaphore_wait(bar, NSP - 1 + 2)
 
     def send_x(n, dz, p):
         j = n * PLANE + p
         remote(sx.at[:, j], gy.at[0, :, j], d_send, d_recv.at[n], ahead(dz, p) + (y,))
 
-    local(sx.at[:, 0], gy.at[0, :, 0], self_sem.at[0])
+    gy[0, :, 0] = sx[:, 0]
     to_all(send_x)
-
-    local(fsend.at[plane], frecv.at[0], self_sem.at[5])
-    for e in range(2):
-        for u in range(2):
-            zb[e, u, 0] = jnp.zeros((32, T), BF)
-    to_all(send_fade)
-    send_plane(sstw, 0)
-
-    for p in range(1, PLANE):
-        remote(ga.at[0], ga.at[p], ga_send, ga_recv, ahead(0, p) + (y,))
 
     def chunk(d, n):
         return gy.at[d, :, pl.ds(PLANE * n, PLANE)]
@@ -356,15 +344,14 @@
     def forward(n):
         if n % 2 == 0:
             wait(chunk(1, n), yl_recv.at[n])
-            remote(chunk(1, n), chunk(2, n), y_send, yo_recv.at[n], right)
+            remote(chunk(1, n), chunk(2, n), y_send, yo_recv.at[n // GC], right)
         else:
             wait(chunk(3, n), yr_recv.at[n])
-            remote(chunk(3, n), chunk(2, n), y_send, yo_recv.at[n], left)
+            remote(chunk(3, n), chunk(2, n), y_send, yo_recv.at[n // GC], left)
 
     def arrived(n):
         if n == 0:
             wait(gy.at[0, :, pl.ds(1, PLANE - 1)], d_recv.at[0])
-            wait(gy.at[0, :, 0], self_sem.at[0])
         else:
             wait(chunk(0, n), d_recv.at[n])
         remote(chunk(0, n), chunk(1, n), y_send, yl_recv.at[n], right)
@@ -376,8 +363,8 @@
                 wait(chunk(1, n), yl_recv.at[n])
             if d == 3 and n % 2 == 0:
                 wait(chunk(3, n), yr_recv.at[n])
-            if d == 2:
-                wait(chunk(2, n), yo_recv.at[n])
+        if d == 2:
+            wait(gy.at[2, :, pl.ds(GJ * g, GJ)], yo_recv.at[g])
 
     r3 = iota((GJ, 8, T), 1)
 
@@ -458,47 +445,48 @@
     def hi(g):
         return pl.ds(GJ * g + HJ, HJ)
 
+    def group(g):
+        return pl.ds(GJ * g, GJ)
+
     def far_partials(g):
         packed(g, 2, put_send(2))
-        remote(ps.at[1, :, lo(g)], hl.at[g], rs_send, rs_recv.at[6 * g], right)
-        remote(ps.at[1, :, hi(g)], hr.at[g], rs_send, rs_recv.at[6 * g + 1], left)
+        remote(ps.at[1, :, lo(g)], hl.at[g], rs_send, rs_recv.at[3 * g], right)
+        remote(ps.at[1, :, hi(g)], hr.at[g], rs_send, rs_recv.at[3 * g + 1], left)
 
     def right_partials(g):
         packed(g, 3, put_send(3))
-        remote(ps.at[2, :, hi(g)], nl.at[:, hi(g)], rs_send, rs_recv.at[6 * g + 2], right)
+        remote(ps.at[2, :, hi(g)], nl.at[:, hi(g)], rs_send, rs_recv.at[3 * g + 2], right)
 
     def left_partials(g):
         packed(g, 1, put_send(1))
-        remote(ps.at[0, :, lo(g)], nr.at[:, lo(g)], rs_send, rs_recv.at[6 * g + 3], left)
+        remote(ps.at[0, :, lo(g)], nr.at[:, lo(g)], rs_send, rs_recv.at[3 * g + 2], left)
 
     def merge(g):
-        wait(hl.at[g], rs_recv.at[6 * g])
+        wait(hl.at[g], rs_recv.at[3 * g])
         for k in range(3):
             mrg[0, g, k] = (ps[2, k, lo(g)].astype(F32) + hl[g, k].astype(F32)).astype(BF)
-        remote(mrg.at[0, g], nl.at[:, lo(g)], rs_send, rs_recv.at[6 * g + 4], right)
-        wait(hr.at[g], rs_recv.at[6 * g + 1])
+        remote(mrg.at[0, g], nl.at[:, lo(g)], rs_send, rs_recv.at[3 * g + 2], right)
+        wait(hr.at[g], rs_recv.at[3 * g + 1])
         for k in range(3):
             mrg[1, g, k] = (ps[0, k, hi(g)].astype(F32) + hr[g, k].astype(F32)).astype(BF)
-        remote(mrg.at[1, g], nr.at[:, hi(g)], rs_send, rs_recv.at[6 * g + 5], left)
+        remote(mrg.at[1, g], nr.at[:, hi(g)], rs_send, rs_recv.at[3 * g + 2], left)
 
     def send_back(n, dz, p):
         j = n * PLANE + p
         remote(ret.at[:, j], rr.at[:, j], ret_send, ret_recv.at[n // GC], behind(dz, p) + (y,))
 
     def give_back(g):
-        wait(nl.at[:, hi(g)], rs_recv.at[6 * g + 2])
-        wait(nr.at[:, lo(g)], rs_recv.at[6 * g + 3])
-        wait(nl.at[:, lo(g)], rs_recv.at[6 * g + 4])
-        wait(nr.at[:, hi(g)], rs_recv.at[6 * g + 5])
+        wait(ps.at[pl.ds(0, 2), :, group(g)], rs_recv.at[3 * g + 2])
         js = pl.ds(GJ * g, GJ)
         for k in range(3):
-            ret[k, js] = (
+            total = (
                 own[k, pl.ds(GR * g, GR)].reshape(GJ, 8, T)
                 + nl[k, js].astype(F32)
                 + nr[k, js].astype(F32)
-            ).astype(BF)
+            )
+            ret[k, js] = total.astype(BF)
         if g == 0:
-            local(ret.at[:, 0], rr.at[:, 0], self_sem.at[6])
+            rr[:, 0] = ret[:, 0]
         to_all(send_back, GC * g, GC * g + GC)
 
     def partials(g):
@@ -539,9 +527,6 @@
     expert_in(1, 1)
     expert_in(1, 3)
     arrived(5)
-    fades_here()
-    plane_totals(0, 0)
-    plane_totals(0, 1)
     forward(4)
     merge(0)
     expert_in(1, 2)
@@ -550,8 +535,11 @@
     arrived(6)
     forward(5)
     arrived(7)
-    spread(0, 0, wsw)
-    spread(0, 1, wsw)
+    frecv[0] = fsend[plane]
+    to_all(send_fade)
+    send_plane(sstw, 0)
+    for p in range(1, PLANE):
+        remote(ga.at[0], ga.at[p], ga_send, ga_recv, ahead(0, p) + (y,))
     forward(6)
     expert_in(2, 0)
     expert_in(2, 1)
@@ -561,6 +549,9 @@
     expert_in(2, 2)
     partials(2)
     own_partials(1)
+    fades_here()
+    plane_totals(0, 0)
+    plane_totals(0, 1)
     expert_in(3, 0)
     expert_in(3, 1)
     expert_in(3, 3)
@@ -578,6 +569,8 @@
     give_back(2)
     weight_grad(3)
     give_back(3)
+    spread(0, 0, wsw)
+    spread(0, 1, wsw)
 
     for n in range(4, 6):
         weight_grad(n)
@@ -589,7 +582,6 @@
     for g in range(GROUPS):
         if g == 0:
             wait(rr.at[:, pl.ds(1, GJ - 1)], ret_recv.at[0])
-            wait(rr.at[:, 0], self_sem.at[6])
         else:
             wait(rr.at[:, pl.ds(GJ * g, GJ)], ret_recv.at[g])
         cs = slice(GR * g, GR * g + GR)
@@ -630,9 +622,26 @@
         for p in range(1, PLANE):
             zz, xx, cc = ahead(0, p)
             remote(
-                lt.at[pair, xx * NC + cc], rtm.at[pair, :, pl.ds(T * p, T)], rt_send, rt_recv,
+                lt.at[pair, xx * NC + cc], rtm.at[pair, :, pl.ds(T * p, T)], rt_send, rt_recv.at[d],
                 (zz, xx, cc, y),
             )
+        rtm[pair, :, 0:T] = lt[pair, plane]
+
+    def projection(d):
+        yy = lax.rem(y + NY - d, NY)
+        pair = pl.ds(yy * 2, 2)
+        wait(rtm.at[pair, :, pl.ds(T, T * (PLANE - 1))], rt_recv.at[d])
+        pg = dot(rtm[pair].reshape(64, 1024), ga[...].reshape(1024, W)).reshape(2, 32, W)
+        pgown[pair] = pg
+        pgs[pair] = pg.astype(BF)
+        for k in range(2):
+            zz = yy * 2 + k
+
+            @pl.when(zz != z)
+            def _():
+                remote(
+                    pgs.at[zz], zr.at[lax.rem(zz + NZ - z, NZ)], z_send, z_recv, (zz, x, c, y)
+                )
 
     out_part(0)
     weight_grad(6)
@@ -663,7 +672,6 @@
     states(srt, dfs, sstr)
     send_plane(sstr, 1)
     transposed(2)
-    local(lt.at[:, plane], rtm.at[:, :, pl.ds(0, T)], self_sem.at[7])
     og_o[...] = (odf * ms[...].astype(F32) * (sig * (1.0 + ogf * (1.0 - sig)))).astype(BF)
 
     wsum = None
@@ -680,6 +688,8 @@
         a = dot(lst[2 * k], dl[:, cols])
         b = dot(lst[2 * k + 1], dl[:, cols])
         vint[:, cols] = jnp.where(half, a, b)
+    wait(ga.at[pl.ds(1, PLANE - 1)], ga_recv)
+    projection(0)
     plane_totals(1, 0)
     plane_totals(1, 1)
     got_states(wsw, 0)
@@ -687,16 +697,9 @@
         rgrad = rgrad + dot(dfi[h], wsw[h], 1, 1)
     rg_o[...] = rgrad.astype(BF)
 
-    wait(ga.at[pl.ds(1, PLANE - 1)], ga_recv)
-    wait(rtm.at[:, :, pl.ds(T, T * (PLANE - 1))], rt_recv)
-    wait(rtm.at[:, :, pl.ds(0, T)], self_sem.at[7])
-    pg = dot(rtm[...].reshape(256, 1024), ga[...].reshape(1024, W))
-    pgown[...] = pg.reshape(8, 32, W)
-    pgs[...] = pg.reshape(8, 32, W).astype(BF)
-    for dz in (1, 7, 2, 6, 3, 5, 4):
-        zz = lax.rem(z + dz, NZ)
-        remote(pgs.at[zz], zr.at[dz], z_send, z_recv, (zz, x, c, y))
-
+    projection(1)
+    projection(3)
+    projection(2)
     spread(1, 0, wsr)
     spread(1, 1, wsr)
     got_states(wsr, 1)
@@ -722,10 +725,9 @@
     wait(ps, rs_send)
     wait(ret.at[:, pl.ds(1, NSP - 1)], ret_send)
     wait(lg.at[pl.ds(0, 3)], lg_send)
-    for k in range(4):
-        wait(inb.at[k // 2, k % 2, pl.ds(1, PLANE - 1)], st_send.at[3 * k])
-        wait(zb.at[k // 2, k % 2, pl.ds(1, NZ - 1)], st_send.at[3 * k + 1])
-        wait(inb.at[k // 2, k % 2, pl.ds(1, PLANE - 1)], st_send.at[3 * k + 2])
+    wait(inb.at[:, :, pl.ds(1, PLANE - 1)], st_send.at[0])
+    wait(zb.at[:, :, pl.ds(1, NZ - 1)], st_send.at[1])
+    wait(outb.at[:, :, pl.ds(1, PLANE - 1)], st_send.at[2])
     wait(frecv.at[pl.ds(1, NSP - 1)], fade_send)
     wait(ga.at[pl.ds(1, PLANE - 1)], ga_send)
     wait(rtm.at[:, :, pl.ds(T, T * (PLANE - 1))], rt_send)
@@ -808,27 +810,24 @@
     bf(8, 32, W),
     fl(8, 32, W),
     sem(14),
-    sem(9),
-    sem(4),
-    sem(4),
     pltpu.SemaphoreType.DMA,
     sem(8),
     pltpu.SemaphoreType.DMA,
     sem(8),
     sem(8),
-    sem(8),
-    pltpu.SemaphoreType.DMA,
-    sem(6 * GROUPS),
-    pltpu.SemaphoreType.DMA,
     sem(GROUPS),
     pltpu.SemaphoreType.DMA,
+    sem(3 * GROUPS),
+    pltpu.SemaphoreType.DMA,
+    sem(GROUPS),
+    pltpu.SemaphoreType.DMA,
     sem(6),
+    sem(3),
     sem(12),
-    sem(12),
-    pltpu.SemaphoreType.DMA,
-    pltpu.SemaphoreType.DMA,
-    pltpu.SemaphoreType.DMA,
-    pltpu.SemaphoreType.DMA,
+    pltpu.SemaphoreType.DMA,
+    pltpu.SemaphoreType.DMA,
+    pltpu.SemaphoreType.DMA,
+    sem(4),
     pltpu.SemaphoreType.DMA,
     pltpu.SemaphoreType.DMA,
 )

time: 99 us -> 97.8 us (0.988)
  no operation moved by 1% of the time
where the time goes in v4:
time: 97.8 us; the launch traced here: 97.4 us
  Pallas kernels  96.6 us (99%)
    pallas_call x1, Pallas kernels, on_device(): pl.pallas_call(body, name='layer_backward', out_shape=tuple((pltpu.VMEM(s...  94.8 us

profile of v4, /device:TPU:24, one launch (start us, length us, event | category | flops | bytes accessed | tf_op | source)
XLA Modules:
  0.0 97.4 jit_solution(11307318825412703960)
XLA Ops:
  0.6 94.8 %layer_backward.1 = (bf16[1,2048,256]{2,1,0:T(8,128)(2,1)S(1)}, bf16[1,2048,256]{2,1,0:T(8,128)(2,1)S(1)}, bf16[1,256,2048]{2,1,0:T(8,128)(2,1)S(1)}, f32[32,512...) custom-call(bf16[128,512]{1,0:T(8,128)(2,1)} %li_h.1, ...), custom_call_target="tpu_custom_call" | custom-call | tf_op jit(solution)/shard_map/layer_backward/pallas_call | solution.py:846
  95.4 1.9 %store.1 = (bf16[1,2048,256]{2,1,0:T(8,128)(2,1)}, bf16[1,2048,256]{2,1,0:T(8,128)(2,1)}, bf16[1,256,2048]{2,1,0:T(8,128)(2,1)}, f32[32,512]{1,0:T(8,128)}, bf16...) custom-call(bf16[1,2048,256]{2,1,0:T(8,128)(2,1)S(1)} %get-tuple-element.1, ...), custom_call_target="tpu_custom_call" | custom-call | tf_op jit(solution)/shard_map/store/pallas_call | solution.py:871

commit v5 on v4

--- a/solution.py
+++ b/solution.py
@@ -569,8 +569,6 @@
     give_back(2)
     weight_grad(3)
     give_back(3)
-    spread(0, 0, wsw)
-    spread(0, 1, wsw)
 
     for n in range(4, 6):
         weight_grad(n)
@@ -644,6 +642,8 @@
                 )
 
     out_part(0)
+    spread(0, 0, wsw)
+    spread(0, 1, wsw)
     weight_grad(6)
     weight_grad(7)
     wait(lg.at[1, first], lg_recv.at[0])
@@ -667,11 +667,16 @@
     od[...] = delta
     dl[...] = delta.astype(BF)
 
-    sides(lambda k: od[:, 128 * k : 128 * k + 128], dfs, dfi)
+    for h in range(HEADS):
+        v = doubled(od[:, 128 * (h // 2) : 128 * (h // 2) + 128], h)
+        dfs[h] = (v * pltpu.roll(fts[h], 64, 1)).astype(BF)
     srt = sr[...].astype(F32).T.astype(BF)
     states(srt, dfs, sstr)
     send_plane(sstr, 1)
     transposed(2)
+    for h in range(HEADS):
+        v = doubled(od[:, 128 * (h // 2) : 128 * (h // 2) + 128], h)
+        dfi[h] = (v * fts[h]).astype(BF)
     og_o[...] = (odf * ms[...].astype(F32) * (sig * (1.0 + ogf * (1.0 - sig)))).astype(BF)
 
     wsum = None

time: 97.8 us -> 97.8 us (level)
  no operation moved by 1% of the time
where the time goes in v5:
time: 97.8 us; the launch traced here: 97.4 us
  Pallas kernels  96.6 us (99%)
    pallas_call x1, Pallas kernels, on_device(): pl.pallas_call(body, name='layer_backward', out_shape=tuple((pltpu.VMEM(s...  94.8 us

profile of v5, /device:TPU:24, one launch (start us, length us, event | category | flops | bytes accessed | tf_op | source)
XLA Modules:
  0.0 97.4 jit_solution(11670164640066326083)
XLA Ops:
  0.6 94.8 %layer_backward.1 = (bf16[1,2048,256]{2,1,0:T(8,128)(2,1)S(1)}, bf16[1,2048,256]{2,1,0:T(8,128)(2,1)S(1)}, bf16[1,256,2048]{2,1,0:T(8,128)(2,1)S(1)}, f32[32,512...) custom-call(bf16[128,512]{1,0:T(8,128)(2,1)} %li_h.1, ...), custom_call_target="tpu_custom_call" | custom-call | tf_op jit(solution)/shard_map/layer_backward/pallas_call | solution.py:851
  95.4 1.9 %store.1 = (bf16[1,2048,256]{2,1,0:T(8,128)(2,1)}, bf16[1,2048,256]{2,1,0:T(8,128)(2,1)}, bf16[1,256,2048]{2,1,0:T(8,128)(2,1)}, f32[32,512]{1,0:T(8,128)}, bf16...) custom-call(bf16[1,2048,256]{2,1,0:T(8,128)(2,1)S(1)} %get-tuple-element.1, ...), custom_call_target="tpu_custom_call" | custom-call | tf_op jit(solution)/shard_map/store/pallas_call | solution.py:876
